TPU v7x, 256 devices: a whole 4x4x8 slice. The times are simulated.
256 devices in a mesh: sp: 32 (over z, x), tp: 8 (over y, core).
Axes of the slice: x: 4, y: 4, z: 8, core: 2. Of those that a mesh axis runs over, the one named last changes fastest.
Arguments:
- prompt_tokens: bfloat16 [65536, 2048], P(('sp', 'tp')), may hold values from -8 to 8
- key_weight: bfloat16 [2048, 2048], P(None, 'tp'), may hold values from -0.125 to 0.125
- value_weight: bfloat16 [2048, 4096], P(None, 'tp'), may hold values from -0.125 to 0.125
- input_weight: bfloat16 [2048, 32], replicated, may hold values from -4 to 4
- forget_weight: bfloat16 [2048, 32], replicated, may hold values from -0.125 to 0.125
- forget_bias: float32 [32], replicated, as said below
- new_token: bfloat16 [2048], replicated, may hold values from -8 to 8
- new_query: bfloat16 [2048], P('tp'), may hold values from -6 to 6
Outputs:
- key_cache: bfloat16 [65536, 2048], P('sp', 'tp')
- value_cache: bfloat16 [65536, 4096], P('sp', 'tp')
- cache_weight: float32 [32, 65536], P('tp', 'sp')
- reading: float32 [4096], P('tp')
Inputs may be any that keep to these rules, and one draw needn't show every extreme that they name: `forget_bias`: every head's forget gate offset is 2 or more.
All inputs are finite; a program needn't handle non-finite values.
Results may differ from a plain program's by a relative error of at most 0.0058.
Values may be sent and summed in bfloat16 or wider, within the bound.
A program may use at most 64 MiB of HBM per device.

v0:
```python
import functools
import math

import jax
import jax.numpy as jnp
from jax import lax
from jax.sharding import Mesh
from jax.sharding import PartitionSpec as P

DQK = 64
DV = 128
SP = ("sp_0", "sp_1")
SP_TP = ("sp_0", "sp_1", "tp")


def sent_to_all(array, axis):
    peers = lax.axis_size(axis)
    return lax.all_to_all(
        jnp.broadcast_to(array[None], (peers, *array.shape)), axis, 0, 0, tiled=True
    )


def joined_by_halves(pieces, combine):
    while len(jax.tree.leaves(pieces)[0]) > 1:
        pieces = jax.vmap(combine)(*(pieces[side::2] for side in (0, 1)))
    return pieces[0]


def entering(array, axis, combine, identity):
    peers, here = (lax.axis_size(axis), lax.axis_index(axis))
    passed = jnp.arange(peers) > here

    def kept(part, zero, own):
        part = jnp.where(
            passed.reshape(-1, *(1 for _ in own.shape)), part, jnp.asarray(zero, own.dtype)
        )
        return part[::-1]

    pieces = sent_to_all(array, axis)
    return joined_by_halves(kept(pieces, identity, array), combine)


def over_copies(array, axis):
    return sent_to_all(array, axis).max(axis=0)


def one_axis_at_a_time(array, axes):
    return functools.reduce(lax.psum, axes, array)


def add_pairs(earlier, later_part):
    return earlier + later_part


def body(
    prompt_tokens,
    key_weight,
    value_weight,
    input_weight,
    forget_weight,
    forget_bias,
    new_token,
    new_query,
):
    heads_dev = key_weight.shape[1] // DQK
    head_start = lax.axis_index("tp") * heads_dev
    gate_input = lax.dynamic_slice_in_dim(input_weight, head_start, heads_dev, 1)
    gate_forget = lax.dynamic_slice_in_dim(forget_weight, head_start, heads_dev, 1)
    forget_shift = lax.dynamic_slice_in_dim(forget_bias, head_start, heads_dev, 0)
    packed = jnp.concatenate([key_weight, value_weight, gate_input, gate_forget], axis=1)
    key_end = heads_dev * DQK
    value_end = heads_dev * (DQK + DV)
    projected = jnp.dot(
        lax.all_gather(prompt_tokens, "tp", axis=0, tiled=True),
        packed,
        preferred_element_type=jnp.float32,
    )
    key_cache = projected[:, :key_end].astype(jnp.bfloat16)
    value_cache = projected[:, key_end:value_end].astype(jnp.bfloat16)
    input_gate = projected[:, value_end : value_end + heads_dev]
    forget_pre = projected[:, value_end + heads_dev :]
    log_forget = jax.nn.log_sigmoid(forget_pre + forget_shift)
    block_total = jnp.sum(log_forget, axis=0)
    carried = entering(block_total, SP, add_pairs, jnp.zeros_like(block_total))
    log_weight = (
        input_gate + (block_total[None, :] - jnp.cumsum(log_forget, axis=0)) + carried[None, :]
    )
    peak_log = over_copies(jnp.max(log_weight, axis=0), SP)
    cache_weight = jnp.transpose(jnp.exp(log_weight - peak_log[None, :]), (1, 0))
    new_key = jnp.dot(new_token, key_weight, preferred_element_type=jnp.float32).astype(
        jnp.bfloat16
    )
    new_value = jnp.dot(new_token, value_weight, preferred_element_type=jnp.float32).astype(
        jnp.bfloat16
    )
    new_gate = jnp.dot(new_token, gate_input, preferred_element_type=jnp.float32)
    new_forget = jax.nn.log_sigmoid(
        jnp.dot(new_token, gate_forget, preferred_element_type=jnp.float32) + forget_shift
    )
    stable_level = jnp.maximum(new_forget + peak_log, new_gate)
    rows = log_weight.shape[0]
    query_heads = new_query.reshape(heads_dev, DQK)
    key_heads = key_cache.reshape(rows, heads_dev, DQK)
    key_score = jnp.einsum(
        "shd,hd->sh", key_heads, query_heads, preferred_element_type=jnp.float32
    ) / math.sqrt(DQK)
    new_score = jnp.einsum(
        "hd,hd->h", new_key.reshape(heads_dev, DQK), query_heads, preferred_element_type=jnp.float32
    ) / math.sqrt(DQK)
    weighted = jnp.exp(new_forget[None, :] + log_weight - stable_level[None, :]) * key_score
    value_heads = value_cache.reshape(rows, heads_dev, DV)
    numer_part = jnp.einsum(
        "sh,she->he", weighted.astype(jnp.bfloat16), value_heads, preferred_element_type=jnp.float32
    )
    denom_part = jnp.sum(weighted, axis=0)
    numerator, denominator = (
        one_axis_at_a_time(numer_part, SP),
        one_axis_at_a_time(denom_part, SP),
    )
    own_term = jnp.exp(new_gate - stable_level) * new_score
    numerator = numerator + own_term[:, None] * new_value.reshape(heads_dev, DV).astype(jnp.float32)
    denominator = denominator + own_term
    reading = numerator / jnp.maximum(jnp.abs(denominator), 1.0)[:, None]
    return (key_cache, value_cache, cache_weight, reading.reshape(-1))


def solution(mesh):
    torus = Mesh(mesh.devices.reshape(8, 4, mesh.shape["tp"]), ("sp_0", "sp_1", "tp"))
    return jax.shard_map(
        body,
        mesh=torus,
        in_specs=(P(SP_TP, None), P(None, "tp"), P(None, "tp"), P(), P(), P(), P(), P("tp")),
        out_specs=(P(SP, "tp"), P(SP, "tp"), P("tp", SP), P("tp")),
        check_vma=False,
    )
```

profile of v0, /device:TPU:32, one launch (start us, length us, event | category | flops | bytes accessed | tf_op | source)
XLA Modules:
  0.0 150.7 jit_solution(6341841162287460119)
XLA Ops:
  7.2 0.0 copy-start.1
  7.2 0.0 copy-start
  7.2 0.0 all-gather.2.cloned.1.call-start
  7.2 0.7 all-gather.2.cloned.1.call-update
  7.9 0.9 reshape.65
  8.8 0.7 reshape.85
  9.6 0.7 reshape.70
  10.3 1.5 fusion.27
  11.8 0.1 reshape.67
  11.8 0.7 dynamic_slice.11
  12.6 0.8 constant_dynamic-slice_fusion
  13.4 1.1 copy.31
  14.4 1.1 copy.30
  15.5 0.1 fusion.17
  15.6 0.1 fusion.19
  15.7 2.0 %fusion.28 = f32[1,512]{1,0:T(1,128)S(1)} fusion(bf16[2048,1]{0,1:T(2,128)(2,1)S(1)} %reshape.70, bf16[2048,512]{1,0:T(8,128)(2,1)} %param.10), kind=kOutput, calls=%fused_computation.52 | convolution fusion | flops 2097152 | bytes 2103296 | tf_op jit(solution)/shard_map/dot_general | solution.py:93
  17.7 47.0 %all-gather.2.cloned.1.call-done = bf16[2048,2048]{1,0:T(8,128)(2,1)} async-done(((bf16[256,2048]{1,0:T(8,128)(2,1)}), bf16[2048,2048]{1,0:T(8,128)(2,1)}) %all-gather.2.cloned.1.call-update) | async-done | bytes 8388624 | tf_op jit(solution)/shard_map/all_gather | solution.py:74
  64.7 0.0 copy-done.1
  64.7 0.0 copy-done
  64.7 14.0 %fusion.25 = (bf16[2048,776]{0,1:T(8,128)(2,1)}, f32[2048,776]{0,1:T(8,128)S(1)}) fusion(bf16[2048,2048]{1,0:T(8,128)(2,1)} %all-gather.2.cloned.1.call-done, bf16[2048,4]{1,0:T(8,128)(2,1)} %copy.31, bf16[2048,4]{1,0:T(8,128)(2,1)} %copy.30, bf16[2048,512]{1,0:T(8,128)(2,1)S(1)} %copy-done, bf16[2048,256]{1,0:T(8,128)(2,1)S(1)} %copy-done.1), kind=kOutput, calls=%fused_computation.49 | convolution fusion | flops 6523863040 | bytes 21102592 | tf_op jit(solution)/shard_map/dot_general | solution.py:73
  78.7 0.0 copy-start.2
  78.7 0.2 fusion.24
  79.0 2.4 %copy-done.2 = f32[2048,776]{0,1:T(8,128)} copy-done((f32[2048,776]{0,1:T(8,128)}, f32[2048,776]{0,1:T(8,128)S(1)}, u32[]{:S(2)}) %copy-start.2) | copy-done | bytes 6357016
  81.4 0.6 broadcast_in_dim.17
  82.0 10.0 %all-to-all-start = ((f32[32,1,4]{2,1,0:T(1,128)}), f32[32,1,4]{2,1,0:T(1,128)S(1)}, u32[]{:S(2)}, u32[]{:S(2)}) async-start(f32[32,1,4]{2,1,0:T(1,128)} %broadcast_in_dim.17), calls=%async_computation | async-start | bytes 32768 | tf_op jit(solution)/shard_map/all_to_all | solution.py:18
  92.1 1.2 reduce-window.6
  93.3 0.2 slice_reduce_fusion
  93.4 0.2 reduce-window.9
  93.6 0.1 add_bitcast_fusion
  93.7 1.3 slice.76
  95.0 5.6 %all-to-all-done = f32[32,1,4]{2,1,0:T(1,128)S(1)} async-done(((f32[32,1,4]{2,1,0:T(1,128)}), f32[32,1,4]{2,1,0:T(1,128)S(1)}, u32[]{:S(2)}, u32[]{:S(2)}) %all-to-all-start) | async-done | bytes 544 | tf_op jit(solution)/shard_map/all_to_all | solution.py:18
  100.6 0.1 copy.32
  100.7 0.1 slice.66
  100.8 0.1 slice.64
  100.9 0.1 slice.65
  101.0 0.1 slice.67
  101.1 0.1 slice.69
  101.2 0.1 slice.68
  101.3 0.1 slice.71
  101.4 0.1 slice.70
  101.5 0.1 slice.73
  101.6 0.1 slice.72
  101.7 0.2 add_reduce_fusion
  101.9 1.0 fusion.22
  103.0 0.6 broadcast_in_dim.19
  103.6 4.9 %all-to-all-start.1 = ((f32[32,1,4]{2,1,0:T(1,128)}), f32[32,1,4]{2,1,0:T(1,128)S(1)}, u32[]{:S(2)}, u32[]{:S(2)}) async-start(f32[32,1,4]{2,1,0:T(1,128)} %broadcast_in_dim.19), calls=%async_computation.1 | async-start | bytes 32768 | tf_op jit(solution)/shard_map/all_to_all | solution.py:18
  108.5 0.2 fusion.26
  108.7 1.8 %slice.77 = bf16[2048,512]{0,1:T(8,128)(2,1)S(1)} slice(bf16[2048,776]{0,1:T(8,128)(2,1)} %get-tuple-element.37), slice={[0:2048], [256:768]} | slice | bytes 4194304 | tf_op jit(solution)/shard_map/slice | solution.py:79
  110.6 1.3 copy.34
  111.9 2.5 %copy.35 = bf16[2048,512]{1,0:T(8,128)(2,1)} copy(bf16[2048,512]{0,1:T(8,128)(2,1)S(1)} %slice.77) | data formatting | bytes 4194304
  114.4 2.7 %all-to-all-done.1 = f32[32,1,4]{2,1,0:T(1,128)S(1)} async-done(((f32[32,1,4]{2,1,0:T(1,128)}), f32[32,1,4]{2,1,0:T(1,128)S(1)}, u32[]{:S(2)}, u32[]{:S(2)}) %all-to-all-start.1) | async-done | bytes 544 | tf_op jit(solution)/shard_map/all_to_all | solution.py:18
  117.1 0.1 reduce_max.19
  117.1 0.1 add_maximum_fusion
  117.3 0.8 fusion.21
  118.1 0.6 fusion.13
  118.7 15.6 %all-reduce = (f32[4,128]{1,0:T(4,128)S(1)}, f32[4]{0:T(128)S(1)}) all-reduce(f32[4,128]{1,0:T(4,128)S(1)} %bitcast.80, f32[4]{0:T(128)S(1)} %get-tuple-element.30), channel_id=1, replica_groups=mesh['sp_0'=8,'sp_1'=4,'tp'=8] {'sp_0'}, use_global_device_ids=true, to_apply=%region_5.6 | all-reduce | flops 516 | bytes 4128 | tf_op jit(solution)/shard_map/psum | solution.py:48
  134.3 8.9 %all-reduce.1 = (f32[4,128]{1,0:T(4,128)S(1)}, f32[4]{0:T(128)S(1)}) all-reduce(f32[4,128]{1,0:T(4,128)S(1)} %get-tuple-element.24, f32[4]{0:T(128)S(1)} %get-tuple-element.25), channel_id=1, replica_groups=mesh['sp_0'=8,'sp_1'=4,'tp'=8] {'sp_1'}, use_global_device_ids=true, to_apply=%region_6.7 | all-reduce | flops 516 | bytes 4128 | tf_op jit(solution)/shard_map/psum | solution.py:48
  143.2 0.7 fusion.18
  (11 shorter events, 0.1 us)
Async XLA Ops:
  7.2 57.6 %copy-start.1 = (bf16[2048,256]{1,0:T(8,128)(2,1)S(1)}, bf16[2048,256]{1,0:T(8,128)(2,1)}, u32[]{:S(2)}) copy-start(bf16[2048,256]{1,0:T(8,128)(2,1)} %param.9) | copy-start | bytes 3145732
  7.2 57.6 %copy-start = (bf16[2048,512]{1,0:T(8,128)(2,1)S(1)}, bf16[2048,512]{1,0:T(8,128)(2,1)}, u32[]{:S(2)}) copy-start(bf16[2048,512]{1,0:T(8,128)(2,1)} %param.10) | copy-start | bytes 6291460
  7.2 57.5 %all-gather.2.cloned.1.call-start = ((), (), s32[]{:S(2)}) async-start(), calls=%async_computation.2 | async-start | bytes 9437184 | tf_op jit(solution)/shard_map/all_gather | solution.py:74
  78.7 2.7 %copy-start.2 = (f32[2048,776]{0,1:T(8,128)}, f32[2048,776]{0,1:T(8,128)S(1)}, u32[]{:S(2)}) copy-start(f32[2048,776]{0,1:T(8,128)S(1)} %get-tuple-element.38) | copy-start | bytes 19070980
  82.0 18.6 %all-to-all-start = ((f32[32,1,4]{2,1,0:T(1,128)}), f32[32,1,4]{2,1,0:T(1,128)S(1)}, u32[]{:S(2)}, u32[]{:S(2)}) async-start(f32[32,1,4]{2,1,0:T(1,128)} %broadcast_in_dim.17), calls=%async_computation | async-start | bytes 32768 | tf_op jit(solution)/shard_map/all_to_all | solution.py:18
  103.6 13.5 %all-to-all-start.1 = ((f32[32,1,4]{2,1,0:T(1,128)}), f32[32,1,4]{2,1,0:T(1,128)S(1)}, u32[]{:S(2)}, u32[]{:S(2)}) async-start(f32[32,1,4]{2,1,0:T(1,128)} %broadcast_in_dim.19), calls=%async_computation.1 | async-start | bytes 32768 | tf_op jit(solution)/shard_map/all_to_all | solution.py:18
Sparse Core Ops, SparseCore 0:
  9.9 54.8 all-gather.1
where the time goes:
time: 151 us
  waiting for transfers between devices  56 us (37%)
  blocking collectives  24.5 us (16%)
  matrix products  18.6 us (12%)
  local copies, waits for them, and re-layouts  17.9 us (12%)
  starting transfers between devices  15 us (10%)
  between operations  14.1 us (9%)
  other arithmetic  4.62 us (3%)
    all_gather x1, waiting for transfers between devices, body(): lax.all_gather(prompt_tokens, 'tp', axis=0, tiled=True)  47 us
    psum x2, blocking collectives, one_axis_at_a_time(): return functools.reduce(lax.psum, axes, array)  24.5 us
    all_to_all x2, starting transfers between devices, sent_to_all(): lax.all_to_all(jnp.broadcast_to(array[None], (peers, *array.shape)), axis...  14.9 us
    dot_general x1, matrix products, body(): jnp.dot(lax.all_gather(prompt_tokens, 'tp', axis=0, tiled=True), packed,...  14 us
    all_to_all x2, waiting for transfers between devices, sent_to_all(): lax.all_to_all(jnp.broadcast_to(array[None], (peers, *array.shape)), axis...  8.31 us
    unnamed x10, local copies, waits for them, and re-layouts  6.94 us
  transfers between devices with their start and end apart: 3, of which 3 were waited for; matrix products, arithmetic and copies ran while one was open for 12% of the time, Pallas kernels for 0%

commit v1 on v0

v1 whole, which is shorter than its diff:
```python
import functools
import math

import jax
import jax.numpy as jnp
from jax import lax
from jax.experimental import pallas as pl
from jax.experimental.pallas import tpu as pltpu
from jax.sharding import Mesh
from jax.sharding import PartitionSpec as P

DQK = 64
DV = 128
SP = ("sp_0", "sp_1")
SP_TP = ("sp_0", "sp_1", "tp")
MESH = pl.DeviceIdType.MESH
F32 = jnp.float32
BF16 = jnp.bfloat16
CHUNK = 32
EARLY = 3


def log_sigmoid(v):
    u = jnp.exp(-jnp.abs(v))
    w = 1.0 + u
    grown = w - 1.0
    tail = jnp.where(grown == 0.0, u, jnp.log(w) * (u / jnp.where(grown == 0.0, 1.0, grown)))
    return -(jnp.maximum(-v, 0.0) + tail)


def remote(src, dst, send, recv, where):
    return pltpu.make_async_remote_copy(
        src_ref=src, dst_ref=dst, send_sem=send, recv_sem=recv, device_id=where, device_id_type=MESH
    )


def kernel(
    tok, kw, vw, iw, fw, fb, nt, nq,
    kout, vout, cwout, rdout,
    xown, xsib, gat, wk, wv, wi, wf,
    sendb, recvb, ngate, nforget, wlog, cpay, cxs, crow, czs, dpay, dxs, drow, dzs, acc, den,
    lsem, own_s, own_r, fwd_s, sib_s, sib_r, osib_s, osib_r,
    b_s, b_r, cx_s, cx_r, cz_s, cz_r, dx_s, dx_r, dz_s, dz_r,
):
    nz, nx, ntp = (lax.axis_size(a) for a in ("sp_0", "sp_1", "tp"))
    z, x, t = (lax.axis_index(a) for a in ("sp_0", "sp_1", "tp"))
    flip = 1 - 2 * (t % 2)
    sib = t + flip
    up, dn = (t + 2) % ntp, (t + ntp - 2) % ntp
    rows = xown.shape[0]
    nchunk = rows // CHUNK

    loads = [
        pltpu.make_async_copy(src, dst, lsem.at[i])
        for i, (src, dst) in enumerate(
            ((tok, xown), (iw, wi), (fw, wf), (kw, wk), (vw, wv))
        )
    ]
    for load in loads:
        load.start()

    barrier = pltpu.get_barrier_semaphore()
    for axis, here, size in (("tp", t, ntp), ("sp_1", x, nx), ("sp_0", z, nz)):
        for d in range(1, size):
            pl.semaphore_signal(
                barrier, inc=1, device_id={axis: (here + d) % size}, device_id_type=MESH
            )
    pl.semaphore_wait(barrier, ntp + nx + nz - 3)

    def own_copies(c):
        piece = xown.at[pl.ds(c * CHUNK, CHUNK)]
        return (
            remote(piece, gat.at[c, pl.ds(0, CHUNK)], own_s.at[0, c], own_r.at[0, c], {"tp": up}),
            remote(
                piece, gat.at[c, pl.ds(CHUNK, CHUNK)], own_s.at[1, c], own_r.at[1, c], {"tp": dn}
            ),
        )

    def send_own(c, carry):
        for copy in own_copies(c):
            copy.start()
        return carry

    def to_sibling(g):
        return remote(
            gat.at[g, pl.ds(0, 2 * CHUNK)],
            gat.at[g, pl.ds(2 * CHUNK, 2 * CHUNK)],
            sib_s.at[g],
            sib_r.at[g],
            {"tp": sib},
        )

    loads[0].wait()
    lax.fori_loop(0, EARLY, send_own, 0)
    own_to_sib = remote(xown, xsib, osib_s, osib_r, {"tp": sib})
    own_to_sib.start()

    loads[1].wait()
    loads[2].wait()
    bias = fb[...]
    token16 = jnp.broadcast_to(nt[...], (16, nt.shape[1]))
    xin = xown[...]
    gate = jnp.dot(xin, wi[...], preferred_element_type=F32)
    forget = log_sigmoid(jnp.dot(xin, wf[...], preferred_element_type=F32) + bias)
    gate_t = gate.T
    forget_t = forget.T
    heads = gate_t.shape[0]
    hd = heads // ntp
    later_mask = (
        lax.broadcasted_iota(jnp.int32, (rows, rows), 0)
        > lax.broadcasted_iota(jnp.int32, (rows, rows), 1)
    ).astype(F32).astype(BF16)
    high = forget_t.astype(BF16)
    rest = forget_t - high.astype(F32)
    mid = rest.astype(BF16)
    low = (rest - mid.astype(F32)).astype(BF16)
    suffix = (
        jnp.dot(low, later_mask, preferred_element_type=F32)
        + jnp.dot(mid, later_mask, preferred_element_type=F32)
        + jnp.dot(high, later_mask, preferred_element_type=F32)
    )
    logw = gate_t + suffix
    total = jnp.broadcast_to(suffix[:, 0:1] + forget_t[:, 0:1], (heads, rows))
    new_g = jnp.dot(token16, wi[...], preferred_element_type=F32)
    new_f = log_sigmoid(jnp.dot(token16, wf[...], preferred_element_type=F32) + bias)
    new_gt = jnp.broadcast_to(new_g.T[:, 0:1], (heads, 128))
    new_ft = jnp.broadcast_to(new_f.T[:, 0:1], (heads, 128))
    for j in range(ntp):
        pick = slice(j * hd, (j + 1) * hd)
        sendb[j, 0:hd, :] = logw[pick]
        sendb[j, hd : 2 * hd, :] = total[pick]
        ngate[j, 0:hd, :] = new_gt[pick]
        ngate[j, hd : 2 * hd, :] = new_gt[pick]
        nforget[j, 0:hd, :] = new_ft[pick]
        nforget[j, hd : 2 * hd, :] = new_ft[pick]

    def across(src, dst_slots, here, size, axis, send, recv):
        copies = []
        for d in range(1, size):
            to = (here + d) % size
            copies.append(
                remote(src(to), dst_slots.at[here], send.at[d - 1], recv.at[d - 1], {axis: to})
            )
        for copy in copies:
            copy.start()
        return copies

    b_copies = across(lambda to: sendb.at[to], recvb, t, ntp, "tp", b_s, b_r)
    recvb[t] = sendb[t]
    lax.fori_loop(EARLY, nchunk, send_own, 0)

    def project(lhs):
        k = jnp.dot(lhs, wk[...], preferred_element_type=F32).astype(BF16)
        v = jnp.dot(lhs, wv[...], preferred_element_type=F32).astype(BF16)
        return k, v

    loads[3].wait()
    loads[4].wait()
    new_k, new_v = project(token16)

    def whole_block(src, source):
        k, v = project(src[...])
        at = pl.ds(pl.multiple_of(source * rows, rows), rows)
        kout[at, :] = k
        vout[at, :] = v

    whole_block(xown, t)

    for copy in b_copies:
        copy.wait_recv()
    zero = jnp.zeros((hd, 128), F32)
    later = zero
    best = None
    for s in reversed(range(ntp)):
        tile = recvb[s]
        for half in (1, 0):
            part = tile[0:hd, half * 128 : (half + 1) * 128] + later
            wlog[2 * s + half, 0:hd, :] = part
            wlog[2 * s + half, hd : 2 * hd, :] = zero
            best = part if best is None else jnp.maximum(best, part)
        later = later + tile[hd : 2 * hd, 0:128]
    block_peak = jnp.broadcast_to(jnp.max(best, axis=1, keepdims=True), (hd, 128))
    cpay[0:hd, :] = later
    cpay[hd : 2 * hd, :] = block_peak
    cx_copies = across(lambda to: cpay, cxs, x, nx, "sp_1", cx_s, cx_r)
    cxs[x] = cpay[...]

    own_to_sib.wait_recv()
    whole_block(xsib, sib)

    for copy in cx_copies:
        copy.wait_recv()

    def scanned(slots, size, here):
        behind = zero
        mine = zero
        peak = None
        for s in reversed(range(size)):
            tile = slots[s]
            candidate = tile[hd : 2 * hd] + behind
            peak = candidate if peak is None else jnp.maximum(peak, candidate)
            mine = mine + jnp.where(s > here, tile[0:hd], zero)
            behind = behind + tile[0:hd]
        return behind, peak, mine

    row_total, row_peak, later_x = scanned(cxs, nx, x)
    crow[0:hd, :] = row_total
    crow[hd : 2 * hd, :] = row_peak
    cz_copies = across(lambda to: crow, czs, z, nz, "sp_0", cz_s, cz_r)
    czs[z] = crow[...]

    def ship(g):
        pltpu.make_async_copy(gat.at[g, pl.ds(0, CHUNK)], gat.at[g, pl.ds(0, CHUNK)], own_r.at[0, g]).wait()
        pltpu.make_async_copy(gat.at[g, pl.ds(0, CHUNK)], gat.at[g, pl.ds(0, CHUNK)], own_r.at[1, g]).wait()
        to_sibling(g).start()

    def forward(g, side):
        half = pl.ds(side * CHUNK, CHUNK)
        return remote(
            gat.at[g, half],
            gat.at[nchunk + g // 2, half],
            fwd_s.at[g],
            own_r.at[side, nchunk + g // 2],
            {"tp": dn if side else up},
        )

    def arrive(g):
        pltpu.make_async_copy(
            gat.at[g, pl.ds(0, 2 * CHUNK)], gat.at[g, pl.ds(0, 2 * CHUNK)], sib_r.at[g]
        ).wait()
        k, v = project(gat[g])
        e = g // nchunk
        c0 = g + e * (g - 2 * nchunk)
        s0 = (t + ntp - 2 - 2 * e) % ntp
        s1 = (t + 2 + 2 * e) % ntp
        starts = (
            s0 * rows + c0 * CHUNK,
            s1 * rows + (c0 + e) * CHUNK,
            (s0 + flip) * rows + c0 * CHUNK,
            (s1 + flip) * rows + (c0 + e) * CHUNK,
        )
        for i, start in enumerate(starts):
            at = pl.ds(pl.multiple_of(start, CHUNK), CHUNK)
            kout[at, :] = k[i * CHUNK : (i + 1) * CHUNK]
            vout[at, :] = v[i * CHUNK : (i + 1) * CHUNK]

    def near(g, carry):
        @pl.when(g < nchunk)
        def _():
            ship(g)

            @pl.when(g % 2 == 0)
            def _():
                forward(g, 0).start()

            @pl.when(g % 2 == 1)
            def _():
                forward(g, 1).start()

        @pl.when(g > 0)
        def _():
            arrive(g - 1)

        return carry

    lax.fori_loop(0, nchunk + 1, near, 0)

    for copy in cz_copies:
        copy.wait_recv()
    _, peak, later_z = scanned(czs, nz, z)
    later = later_x + later_z
    own_gate = ngate[t]
    own_forget = nforget[t]
    peak8 = jnp.concatenate([peak, peak], axis=0)
    stable = jnp.maximum(own_forget + peak8, own_gate)
    shift = own_forget - stable
    for s in range(2 * ntp):
        whole = wlog[s, 0:hd, :] + later
        cwout[:, s * 128 : (s + 1) * 128] = jnp.exp(whole - peak)
        wlog[s, 0:hd, :] = jnp.exp(whole + shift[0:hd])

    query = jnp.broadcast_to(nq[...], (2 * hd, nq.shape[1]))
    lane_head = lax.broadcasted_iota(jnp.int32, query.shape, 1) // DQK
    row_head = lax.broadcasted_iota(jnp.int32, query.shape, 0)
    queries = jnp.where(lane_head == row_head, query.astype(F32), 0.0)
    queries_low = queries.astype(BF16)
    acc[...] = jnp.zeros_like(acc)
    den[...] = jnp.zeros_like(den)

    def read(unit):
        at = pl.ds(pl.multiple_of(unit * 128, 128), 128)
        score = lax.dot_general(
            queries_low, kout[at, :], (((1,), (1,)), ((), ())), preferred_element_type=F32
        ) * (1.0 / math.sqrt(DQK))
        weighted = wlog[unit] * score
        den[...] += weighted
        acc[...] += jnp.dot(weighted.astype(BF16), vout[at, :], preferred_element_type=F32)

    def read_near(i, carry):
        away = (i // 4) + (i // 8)
        read(4 * ((t // 2 + away) % (ntp // 2)) + i % 4)
        return carry

    lax.fori_loop(0, 12, read_near, 0)

    def far(g, carry):
        @pl.when(g < nchunk + nchunk // 2)
        def _():
            ship(g)

        @pl.when(g > nchunk)
        def _():
            arrive(g - 1)

        return carry

    lax.fori_loop(nchunk, nchunk + nchunk // 2 + 1, far, 0)
    opposite = 4 * ((t // 2 + 2) % (ntp // 2))

    def read_far(i, carry):
        read(opposite + i)
        return carry

    lax.fori_loop(0, 4, read_far, 0)

    for h in range(hd):
        dpay[h : h + 1, :] = acc[h : h + 1, h * DV : (h + 1) * DV]
    dpay[hd : 2 * hd, :] = den[0:hd, :]
    dx_copies = across(lambda to: dpay, dxs, x, nx, "sp_1", dx_s, dx_r)
    dxs[x] = dpay[...]
    for copy in dx_copies:
        copy.wait_recv()
    drow[...] = functools.reduce(jnp.add, [dxs[s] for s in range(nx)])
    dz_copies = across(lambda to: drow, dzs, z, nz, "sp_0", dz_s, dz_r)
    dzs[z] = drow[...]
    for copy in dz_copies:
        copy.wait_recv()
    summed = functools.reduce(jnp.add, [dzs[s] for s in range(nz)])
    new_score = jnp.sum(
        queries * new_k[0:1, :].astype(F32), axis=1, keepdims=True
    )[0:hd] * (1.0 / math.sqrt(DQK))
    own_term = jnp.exp(own_gate - stable)[0:hd] * new_score
    values = jnp.concatenate(
        [new_v[0:1, h * DV : (h + 1) * DV].astype(F32) for h in range(hd)], axis=0
    )
    numerator = summed[0:hd] + own_term * values
    denominator = jnp.sum(summed[hd : 2 * hd], axis=1, keepdims=True) + own_term
    rdout[...] = numerator / jnp.maximum(jnp.abs(denominator), 1.0)

    def own_left(c, carry):
        for copy in own_copies(c):
            copy.wait_send()
        return carry

    lax.fori_loop(0, nchunk, own_left, 0)

    def forwards_left(i, carry):
        forward(2 * i, 0).wait_send()
        forward(2 * i + 1, 1).wait_send()
        return carry

    lax.fori_loop(0, nchunk // 2, forwards_left, 0)

    def sibling_left(g, carry):
        to_sibling(g).wait_send()
        return carry

    lax.fori_loop(0, nchunk + nchunk // 2, sibling_left, 0)
    own_to_sib.wait_send()
    for copy in (*b_copies, *cx_copies, *cz_copies, *dx_copies, *dz_copies):
        copy.wait_send()


def body(
    prompt_tokens,
    key_weight,
    value_weight,
    input_weight,
    forget_weight,
    forget_bias,
    new_token,
    new_query,
):
    nz, nx, ntp = (lax.axis_size(a) for a in ("sp_0", "sp_1", "tp"))
    rows, depth = prompt_tokens.shape
    kcols, vcols = key_weight.shape[1], value_weight.shape[1]
    heads = input_weight.shape[1]
    hd = heads // ntp
    assert hd == 4 and ntp == 8 and rows == 256
    nchunk = rows // CHUNK
    groups = nchunk + nchunk // 2
    anywhere = pl.BlockSpec(memory_space=pl.ANY)
    vmem = pl.BlockSpec(memory_space=pltpu.VMEM)
    dma = pltpu.SemaphoreType.DMA
    tile = (2 * hd, 128)
    key_cache, value_cache, cache_weight, reading = pl.pallas_call(
        kernel,
        out_shape=(
            jax.ShapeDtypeStruct((rows * ntp, kcols), BF16),
            jax.ShapeDtypeStruct((rows * ntp, vcols), BF16),
            jax.ShapeDtypeStruct((hd, rows * ntp), F32),
            jax.ShapeDtypeStruct((hd, DV), F32),
        ),
        in_specs=[anywhere] * 5 + [vmem] * 3,
        out_specs=[vmem] * 4,
        scratch_shapes=[
            pltpu.VMEM((rows, depth), BF16),
            pltpu.VMEM((rows, depth), BF16),
            pltpu.VMEM((groups, 4 * CHUNK, depth), BF16),
            pltpu.VMEM((depth, kcols), BF16),
            pltpu.VMEM((depth, vcols), BF16),
            pltpu.VMEM((depth, heads), BF16),
            pltpu.VMEM((depth, heads), BF16),
            pltpu.VMEM((ntp, 2 * hd, rows), F32),
            pltpu.VMEM((ntp, 2 * hd, rows), F32),
            pltpu.VMEM((ntp, *tile), F32),
            pltpu.VMEM((ntp, *tile), F32),
            pltpu.VMEM((2 * ntp, *tile), F32),
            pltpu.VMEM(tile, F32),
            pltpu.VMEM((nx, *tile), F32),
            pltpu.VMEM(tile, F32),
            pltpu.VMEM((nz, *tile), F32),
            pltpu.VMEM(tile, F32),
            pltpu.VMEM((nx, *tile), F32),
            pltpu.VMEM(tile, F32),
            pltpu.VMEM((nz, *tile), F32),
            pltpu.VMEM((2 * hd, vcols), F32),
            pltpu.VMEM(tile, F32),
            dma((5,)),
            dma((2, nchunk)),
            dma((2, groups)),
            dma((nchunk,)),
            dma((groups,)),
            dma((groups,)),
            dma(()),
            dma(()),
            dma((ntp - 1,)),
            dma((ntp - 1,)),
            dma((nx - 1,)),
            dma((nx - 1,)),
            dma((nz - 1,)),
            dma((nz - 1,)),
            dma((nx - 1,)),
            dma((nx - 1,)),
            dma((nz - 1,)),
            dma((nz - 1,)),
        ],
        compiler_params=pltpu.CompilerParams(
            collective_id=0, has_side_effects=True, vmem_limit_bytes=40 * 1024 * 1024
        ),
        name="prefill",
    )(
        prompt_tokens,
        key_weight,
        value_weight,
        input_weight,
        forget_weight,
        forget_bias.reshape(1, -1),
        new_token.reshape(1, -1),
        new_query.reshape(1, -1),
    )
    return key_cache, value_cache, cache_weight, reading.reshape(-1)


def solution(mesh):
    torus = Mesh(mesh.devices.reshape(8, 4, mesh.shape["tp"]), ("sp_0", "sp_1", "tp"))
    return jax.shard_map(
        body,
        mesh=torus,
        in_specs=(P(SP_TP, None), P(None, "tp"), P(None, "tp"), P(), P(), P(), P(), P("tp")),
        out_specs=(P(SP, "tp"), P(SP, "tp"), P("tp", SP), P("tp")),
        check_vma=False,
    )
```

time: 151 us -> 70.9 us (0.47)
  the two profiles are of different devices: /device:TPU:32 before, /device:TPU:1 now
where the time goes in v1:
time: 70.9 us; the launch traced here: 70.6 us
  Pallas kernels  58.1 us (82%)
  local copies, waits for them, and re-layouts  11.9 us (17%)
    pallas_call x1, Pallas kernels, body(): pl.pallas_call(kernel, out_shape=(jax.ShapeDtypeStruct((rows * ntp, kcols...  58.1 us
    unnamed x14, local copies, waits for them, and re-layouts  10.5 us

profile of v1, /device:TPU:1, one launch (start us, length us, event | category | flops | bytes accessed | tf_op | source)
XLA Modules:
  0.0 70.6 jit_solution(6021979432014281304)
XLA Ops:
  0.6 0.7 reshape.22.nq
  1.3 0.7 reshape.21.nt
  2.0 1.2 %copy.12.iw = bf16[2048,32]{1,0:T(8,128)(2,1)S(1)} copy(bf16[2048,32]{0,1:T(8,128)(2,1)} %param.11) | data formatting | bytes 262144 | tf_op args[3]
  3.2 1.2 %copy.13.fw = bf16[2048,32]{1,0:T(8,128)(2,1)S(1)} copy(bf16[2048,32]{0,1:T(8,128)(2,1)} %param.12) | data formatting | bytes 262144 | tf_op args[4]
  4.4 0.0 copy-start
  4.4 1.6 %copy-done = bf16[2048,512]{1,0:T(8,128)(2,1)S(1)} copy-done((bf16[2048,512]{1,0:T(8,128)(2,1)S(1)}, bf16[2048,512]{1,0:T(8,128)(2,1)}, u32[]{:S(2)}) %copy-start) | copy-done | bytes 2097176
  5.9 0.0 copy-start.1
  6.0 1.2 %copy-done.1 = bf16[256,2048]{1,0:T(8,128)(2,1)S(1)} copy-done((bf16[256,2048]{1,0:T(8,128)(2,1)S(1)}, bf16[256,2048]{1,0:T(8,128)(2,1)}, u32[]{:S(2)}) %copy-start.1) | copy-done | bytes 1048600
  7.2 0.0 copy-start.2
  7.2 1.2 %copy-done.2 = bf16[2048,256]{1,0:T(8,128)(2,1)S(1)} copy-done((bf16[2048,256]{1,0:T(8,128)(2,1)S(1)}, bf16[2048,256]{1,0:T(8,128)(2,1)}, u32[]{:S(2)}) %copy-start.2) | copy-done | bytes 1048600
  8.4 0.0 copy-start.3
  8.4 0.7 copy-done.3
  9.1 58.1 %prefill.1 = (bf16[2048,256]{1,0:T(8,128)(2,1)S(1)}, bf16[2048,512]{1,0:T(8,128)(2,1)S(1)}, f32[4,2048]{1,0:T(4,128)S(1)}, f32[4,128]{1,0:T(4,128)S(1)}) custom-call(bf16[256,2048]{1,0:T(8,128)(2,1)S(1)} %copy-done.1, bf16[2048,256]{1,0:T(8,128)(2,1)S(1)} %copy-done.2, bf16[2048,512]{1,0:T(8,128)(2,1)S(1)} %copy-done, bf16[2048,32]{1,0:T(8,128)(2,1)S(1)} %copy.12.iw, ...), custom_call_target="tpu_custom_call" | custom-call | tf_op jit(solution)/shard_map/prefill/pallas_call | solution.py:396
  67.1 1.0 %copy.18 = bf16[2048,256]{1,0:T(8,128)(2,1)} copy(bf16[2048,256]{1,0:T(8,128)(2,1)S(1)} %get-tuple-element.16) | data formatting | bytes 2097152
  68.1 1.3 %copy.19 = bf16[2048,512]{1,0:T(8,128)(2,1)} copy(bf16[2048,512]{1,0:T(8,128)(2,1)S(1)} %get-tuple-element.17) | data formatting | bytes 4194304
  69.4 0.6 copy.20
  70.0 0.6 copy.21
Async XLA Ops:
  4.4 1.6 %copy-start = (bf16[2048,512]{1,0:T(8,128)(2,1)S(1)}, bf16[2048,512]{1,0:T(8,128)(2,1)}, u32[]{:S(2)}) copy-start(bf16[2048,512]{1,0:T(8,128)(2,1)} %vw.1) | copy-start | bytes 6291460
  5.9 1.2 %copy-start.1 = (bf16[256,2048]{1,0:T(8,128)(2,1)S(1)}, bf16[256,2048]{1,0:T(8,128)(2,1)}, u32[]{:S(2)}) copy-start(bf16[256,2048]{1,0:T(8,128)(2,1)} %tok.1) | copy-start | bytes 3145732
  7.2 1.2 %copy-start.2 = (bf16[2048,256]{1,0:T(8,128)(2,1)S(1)}, bf16[2048,256]{1,0:T(8,128)(2,1)}, u32[]{:S(2)}) copy-start(bf16[2048,256]{1,0:T(8,128)(2,1)} %kw.1) | copy-start | bytes 3145732
  8.4 0.7 copy-start.3

commit v2 on v1

--- a/solution.py
+++ b/solution.py
@@ -37,7 +37,7 @@
 def kernel(
     tok, kw, vw, iw, fw, fb, nt, nq,
     kout, vout, cwout, rdout,
-    xown, xsib, gat, wk, wv, wi, wf,
+    xown, xsib, gat, wk, wv, wif, bias_v, token_v, query_v,
     sendb, recvb, ngate, nforget, wlog, cpay, cxs, crow, czs, dpay, dxs, drow, dzs, acc, den,
     lsem, own_s, own_r, fwd_s, sib_s, sib_r, osib_s, osib_r,
     b_s, b_r, cx_s, cx_r, cz_s, cz_r, dx_s, dx_r, dz_s, dz_r,
@@ -53,7 +53,16 @@
     loads = [
         pltpu.make_async_copy(src, dst, lsem.at[i])
         for i, (src, dst) in enumerate(
-            ((tok, xown), (iw, wi), (fw, wf), (kw, wk), (vw, wv))
+            (
+                (tok, xown),
+                (iw, wif.at[pl.ds(0, iw.shape[0])]),
+                (fw, wif.at[pl.ds(iw.shape[0], iw.shape[0])]),
+                (fb, bias_v),
+                (nt, token_v),
+                (nq, query_v),
+                (kw, wk),
+                (vw, wv),
+            )
         )
     ]
     for load in loads:
@@ -95,17 +104,17 @@
     own_to_sib = remote(xown, xsib, osib_s, osib_r, {"tp": sib})
     own_to_sib.start()
 
-    loads[1].wait()
-    loads[2].wait()
-    bias = fb[...]
-    token16 = jnp.broadcast_to(nt[...], (16, nt.shape[1]))
-    xin = xown[...]
-    gate = jnp.dot(xin, wi[...], preferred_element_type=F32)
-    forget = log_sigmoid(jnp.dot(xin, wf[...], preferred_element_type=F32) + bias)
-    gate_t = gate.T
-    forget_t = forget.T
-    heads = gate_t.shape[0]
+    for load in loads[1:6]:
+        load.wait()
+    heads = iw.shape[0]
     hd = heads // ntp
+    depth = xown.shape[1]
+    bias = bias_v[...].reshape(1, heads).T
+    token16 = jnp.broadcast_to(token_v[...].reshape(1, depth), (16, depth))
+    over_lanes = (((1,), (1,)), ((), ()))
+    gates = lax.dot_general(wif[...], xown[...], over_lanes, preferred_element_type=F32)
+    gate_t = gates[0:heads]
+    forget_t = log_sigmoid(gates[heads:] + bias)
     later_mask = (
         lax.broadcasted_iota(jnp.int32, (rows, rows), 0)
         > lax.broadcasted_iota(jnp.int32, (rows, rows), 1)
@@ -121,10 +130,9 @@
     )
     logw = gate_t + suffix
     total = jnp.broadcast_to(suffix[:, 0:1] + forget_t[:, 0:1], (heads, rows))
-    new_g = jnp.dot(token16, wi[...], preferred_element_type=F32)
-    new_f = log_sigmoid(jnp.dot(token16, wf[...], preferred_element_type=F32) + bias)
-    new_gt = jnp.broadcast_to(new_g.T[:, 0:1], (heads, 128))
-    new_ft = jnp.broadcast_to(new_f.T[:, 0:1], (heads, 128))
+    new_gates = lax.dot_general(wif[...], token16, over_lanes, preferred_element_type=F32)
+    new_gt = jnp.broadcast_to(new_gates[0:heads, 0:1], (heads, 128))
+    new_ft = jnp.broadcast_to(log_sigmoid(new_gates[heads:, 0:1] + bias), (heads, 128))
     for j in range(ntp):
         pick = slice(j * hd, (j + 1) * hd)
         sendb[j, 0:hd, :] = logw[pick]
@@ -154,8 +162,8 @@
         v = jnp.dot(lhs, wv[...], preferred_element_type=F32).astype(BF16)
         return k, v
 
-    loads[3].wait()
-    loads[4].wait()
+    loads[6].wait()
+    loads[7].wait()
     new_k, new_v = project(token16)
 
     def whole_block(src, source):
@@ -279,7 +287,7 @@
         cwout[:, s * 128 : (s + 1) * 128] = jnp.exp(whole - peak)
         wlog[s, 0:hd, :] = jnp.exp(whole + shift[0:hd])
 
-    query = jnp.broadcast_to(nq[...], (2 * hd, nq.shape[1]))
+    query = jnp.broadcast_to(query_v[...].reshape(1, -1), (2 * hd, nq.shape[0]))
     lane_head = lax.broadcasted_iota(jnp.int32, query.shape, 1) // DQK
     row_head = lax.broadcasted_iota(jnp.int32, query.shape, 0)
     queries = jnp.where(lane_head == row_head, query.astype(F32), 0.0)
@@ -371,6 +379,15 @@
         copy.wait_send()
 
 
+def put_out(*refs):
+    sems = refs[8]
+    copies = [pltpu.make_async_copy(refs[i], refs[4 + i], sems.at[i]) for i in range(4)]
+    for copy in copies:
+        copy.start()
+    for copy in copies:
+        copy.wait()
+
+
 def body(
     prompt_tokens,
     key_weight,
@@ -389,7 +406,7 @@
     assert hd == 4 and ntp == 8 and rows == 256
     nchunk = rows // CHUNK
     groups = nchunk + nchunk // 2
-    anywhere = pl.BlockSpec(memory_space=pl.ANY)
+    anywhere = pl.BlockSpec(memory_space=pltpu.HBM)
     vmem = pl.BlockSpec(memory_space=pltpu.VMEM)
     dma = pltpu.SemaphoreType.DMA
     tile = (2 * hd, 128)
@@ -401,7 +418,7 @@
             jax.ShapeDtypeStruct((hd, rows * ntp), F32),
             jax.ShapeDtypeStruct((hd, DV), F32),
         ),
-        in_specs=[anywhere] * 5 + [vmem] * 3,
+        in_specs=[anywhere] * 8,
         out_specs=[vmem] * 4,
         scratch_shapes=[
             pltpu.VMEM((rows, depth), BF16),
@@ -409,8 +426,10 @@
             pltpu.VMEM((groups, 4 * CHUNK, depth), BF16),
             pltpu.VMEM((depth, kcols), BF16),
             pltpu.VMEM((depth, vcols), BF16),
-            pltpu.VMEM((depth, heads), BF16),
-            pltpu.VMEM((depth, heads), BF16),
+            pltpu.VMEM((2 * heads, depth), BF16),
+            pltpu.VMEM((heads,), F32),
+            pltpu.VMEM((depth,), BF16),
+            pltpu.VMEM((kcols,), BF16),
             pltpu.VMEM((ntp, 2 * hd, rows), F32),
             pltpu.VMEM((ntp, 2 * hd, rows), F32),
             pltpu.VMEM((ntp, *tile), F32),
@@ -426,7 +445,7 @@
             pltpu.VMEM((nz, *tile), F32),
             pltpu.VMEM((2 * hd, vcols), F32),
             pltpu.VMEM(tile, F32),
-            dma((5,)),
+            dma((8,)),
             dma((2, nchunk)),
             dma((2, groups)),
             dma((nchunk,)),
@@ -450,15 +469,30 @@
         ),
         name="prefill",
     )(
-        prompt_tokens,
-        key_weight,
-        value_weight,
-        input_weight,
-        forget_weight,
-        forget_bias.reshape(1, -1),
-        new_token.reshape(1, -1),
-        new_query.reshape(1, -1),
+        *(
+            pltpu.with_memory_space_constraint(operand, pltpu.HBM)
+            for operand in (
+                prompt_tokens,
+                key_weight,
+                value_weight,
+                input_weight.T,
+                forget_weight.T,
+                forget_bias,
+                new_token,
+                new_query,
+            )
+        )
     )
+    results = (key_cache, value_cache, cache_weight, reading)
+    key_cache, value_cache, cache_weight, reading = pl.pallas_call(
+        put_out,
+        out_shape=tuple(jax.ShapeDtypeStruct(r.shape, r.dtype) for r in results),
+        in_specs=[vmem] * 4,
+        out_specs=[anywhere] * 4,
+        scratch_shapes=[dma((4,))],
+        compiler_params=pltpu.CompilerParams(vmem_limit_bytes=1024 * 1024),
+        name="put_out",
+    )(*results)
     return key_cache, value_cache, cache_weight, reading.reshape(-1)
 
 

time: 70.9 us -> 60.3 us (0.85)
  local copies, waits for them, and re-layouts: 11.9 us -> 0 us
  Pallas kernels: 58.1 us -> 59.6 us
    unnamed x14 -> x0, local copies, waits for them, and re-layouts: 10.5 us -> none
    pallas_call x0 -> x1, Pallas kernels: none -> 1.71 us  [body(): pl.pallas_call(put_out, out_shape=tuple((jax.ShapeDtypeStruct(r.shape, r....]
    reshape x2 -> x0, local copies, waits for them, and re-layouts: 1.35 us -> none  [the longest x1 0.69 us: body(): new_token.reshape(1, -1)]
where the time goes in v2:
time: 60.3 us
  Pallas kernels  59.6 us (99%)
  between operations  0.64 us (1%)
    pallas_call x1, Pallas kernels, body(): pl.pallas_call(kernel, out_shape=(jax.ShapeDtypeStruct((rows * ntp, kcols...  57.9 us
    pallas_call x1, Pallas kernels, body(): pl.pallas_call(put_out, out_shape=tuple((jax.ShapeDtypeStruct(r.shape, r....  1.71 us

profile of v2, /device:TPU:1, one launch (start us, length us, event | category | flops | bytes accessed | tf_op | source)
XLA Modules:
  0.0 60.3 jit_solution(7714471315336261)
XLA Ops:
  0.6 57.9 %prefill.1 = (bf16[2048,256]{1,0:T(8,128)(2,1)S(1)}, bf16[2048,512]{1,0:T(8,128)(2,1)S(1)}, f32[4,2048]{1,0:T(4,128)S(1)}, f32[4,128]{1,0:T(4,128)S(1)}) custom-call(bf16[256,2048]{1,0:T(8,128)(2,1)} %tok.1, bf16[2048,256]{1,0:T(8,128)(2,1)} %kw.1, bf16[2048,512]{1,0:T(8,128)(2,1)} %vw.1, bf16[32,2048]{1,0:T(8,128)(2,1)} %bitcast.3, ...), custom_call_target="tpu_custom_call" | custom-call | tf_op jit(solution)/shard_map/prefill/pallas_call | solution.py:413
  58.6 1.7 %put_out.1 = (bf16[2048,256]{1,0:T(8,128)(2,1)}, bf16[2048,512]{1,0:T(8,128)(2,1)}, f32[4,2048]{1,0:T(4,128)}, f32[4,128]{1,0:T(4,128)}) custom-call(bf16[2048,256]{1,0:T(8,128)(2,1)S(1)} %get-tuple-element.12.refs_0_, bf16[2048,512]{1,0:T(8,128)(2,1)S(1)} %get-tuple-element.13.refs_1_, f32[4,2048]{1,0:T(4,128)S(1)} %get-tuple-element.14.refs_2_, ...), custom_call_target="tpu_custom_call" | custom-call | tf_op jit(solution)/shard_map/put_out/pallas_call | solution.py:487

commit v3 on v2

v3 whole, which is shorter than its diff:
```python
import functools
import math

import jax
import jax.numpy as jnp
from jax import lax
from jax.experimental import pallas as pl
from jax.experimental.pallas import tpu as pltpu
from jax.sharding import Mesh
from jax.sharding import PartitionSpec as P

DQK = 64
DV = 128
SP = ("sp_0", "sp_1")
SP_TP = ("sp_0", "sp_1", "tp")
MESH = pl.DeviceIdType.MESH
F32 = jnp.float32
BF16 = jnp.bfloat16
CHUNK = 32
EARLY = (2, 4)


def log_sigmoid(v):
    u = jnp.exp(-jnp.abs(v))
    w = 1.0 + u
    grown = w - 1.0
    tail = jnp.where(grown == 0.0, u, jnp.log(w) * (u / jnp.where(grown == 0.0, 1.0, grown)))
    return -(jnp.maximum(-v, 0.0) + tail)


def remote(src, dst, send, recv, where):
    return pltpu.make_async_remote_copy(
        src_ref=src, dst_ref=dst, send_sem=send, recv_sem=recv, device_id=where, device_id_type=MESH
    )


def kernel(
    tok, kw, vw, iw, fw, fb, nt, nq,
    kout, vout, cwout, rdout,
    xown, xsib, gat, wk, wv, wif, bias_v, token_v, query_v,
    tmrow, tmall, lwpay, lwall, wread, cpay, cxs, crow, czs, dpay, dxs, drow, dzs, acc, den,
    lsem, own_s, own_r, fwd_s, sib_s, sib_r, osib_s, osib_r,
    tm_s, tm_r, lw_s, lw_r, cx_s, cx_r, cz_s, cz_r, dx_s, dx_r, dz_s, dz_r, near_z,
):
    nz, nx, ntp = (lax.axis_size(a) for a in ("sp_0", "sp_1", "tp"))
    z, x, t = (lax.axis_index(a) for a in ("sp_0", "sp_1", "tp"))
    flip = 1 - 2 * (t % 2)
    sib = t + flip
    up, dn = (t + 2) % ntp, (t + ntp - 2) % ntp
    rows, depth = xown.shape
    nchunk = rows // CHUNK
    groups = gat.shape[0]
    heads = iw.shape[0]
    hd = heads // ntp
    over_lanes = (((1,), (1,)), ((), ()))

    loads = [
        pltpu.make_async_copy(src, dst, lsem.at[i])
        for i, (src, dst) in enumerate(
            (
                (tok, xown),
                (iw, wif.at[pl.ds(0, heads)]),
                (fw, wif.at[pl.ds(heads, heads)]),
                (fb, bias_v),
                (nt, token_v),
                (nq, query_v),
                (kw, wk),
                (vw, wv),
            )
        )
    ]
    for load in loads:
        load.start()

    barrier = pltpu.get_barrier_semaphore()

    def signal(semaphore, axis, to):
        pl.semaphore_signal(semaphore, inc=1, device_id={axis: to}, device_id_type=MESH)

    for d in range(1, ntp):
        signal(barrier, "tp", (t + d) % ntp)
    for d in range(1, nx):
        signal(barrier, "sp_1", (x + d) % nx)
    for d in (1, nz - 1):
        signal(barrier, "sp_0", (z + d) % nz)
    pl.semaphore_wait(barrier, ntp + nx)
    for d in (1, nz - 1):
        signal(near_z.at[0], "sp_0", (z + d) % nz)

    def own_copies(c):
        piece = xown.at[pl.ds(c * CHUNK, CHUNK)]
        return (
            remote(piece, gat.at[c, pl.ds(0, CHUNK)], own_s.at[0, c], own_r.at[0, c], {"tp": up}),
            remote(
                piece, gat.at[c, pl.ds(CHUNK, CHUNK)], own_s.at[1, c], own_r.at[1, c], {"tp": dn}
            ),
        )

    def send_own(c, carry):
        for copy in own_copies(c):
            copy.start()
        return carry

    def across(src, dst_slots, here, size, axis, send, recv):
        copies = []
        for d in range(1, size):
            to = (here + d) % size
            copies.append(
                remote(src(to), dst_slots.at[here], send.at[d - 1], recv.at[d - 1], {axis: to})
            )
        for copy in copies:
            copy.start()
        return copies

    loads[0].wait()
    lax.fori_loop(0, EARLY[0], send_own, 0)
    own_to_sib = remote(xown, xsib, osib_s, osib_r, {"tp": sib})
    own_to_sib.start()

    for load in loads[1:6]:
        load.wait()
    bias = bias_v[...].reshape(1, heads).T
    gates = lax.dot_general(wif[...], xown[...], over_lanes, preferred_element_type=F32)
    gate_t = gates[0:heads]
    forget_t = log_sigmoid(gates[heads:] + bias)
    later_mask = (
        lax.broadcasted_iota(jnp.int32, (rows, rows), 0)
        > lax.broadcasted_iota(jnp.int32, (rows, rows), 1)
    ).astype(F32).astype(BF16)
    high = forget_t.astype(BF16)
    rest = forget_t - high.astype(F32)
    mid = rest.astype(BF16)
    low = (rest - mid.astype(F32)).astype(BF16)
    suffix = (
        jnp.dot(low, later_mask, preferred_element_type=F32)
        + jnp.dot(mid, later_mask, preferred_element_type=F32)
        + jnp.dot(high, later_mask, preferred_element_type=F32)
    )
    logw = gate_t + suffix
    total = suffix[:, 0:1] + forget_t[:, 0:1]
    top = jnp.max(logw, axis=1, keepdims=True)
    lane = lax.broadcasted_iota(jnp.int32, (heads, 128), 1)
    pairs = jnp.concatenate(
        [jnp.where(lane < 64, total, top), jnp.zeros((128 - heads, 128), F32)], axis=0
    ).T
    tmrow[0:1, :] = pairs[0:1]
    tmrow[1:2, :] = pairs[64:65]
    tm_copies = across(lambda to: tmrow, tmall, t, ntp, "tp", tm_s, tm_r)
    tmall[t] = tmrow[...]

    lax.fori_loop(EARLY[0], EARLY[1], send_own, 0)

    pl.semaphore_wait(near_z.at[0], 2)
    for d in (2, nz - 2):
        signal(near_z.at[1], "sp_0", (z + d) % nz)

    def project(lhs):
        k = jnp.dot(lhs, wk[...], preferred_element_type=F32).astype(BF16)
        v = jnp.dot(lhs, wv[...], preferred_element_type=F32).astype(BF16)
        return k, v

    def whole_block(src, source):
        k, v = project(src[...])
        at = pl.ds(pl.multiple_of(source * rows, rows), rows)
        kout[at, :] = k
        vout[at, :] = v

    loads[6].wait()
    loads[7].wait()
    whole_block(xown, t)

    for copy in tm_copies:
        copy.wait_recv()
    block_total = jnp.zeros((1, 128), F32)
    mine = block_total
    block_top = None
    for s in reversed(range(ntp)):
        candidate = tmall[s, 1:2, :] + block_total
        block_top = candidate if block_top is None else jnp.maximum(block_top, candidate)
        mine = mine + jnp.where(s > t, tmall[s, 0:1, :], 0.0)
        block_total = block_total + tmall[s, 0:1, :]
    logw = logw + mine.T[0:heads]

    def twice(a):
        return jnp.concatenate(
            [a[j * hd : (j + 1) * hd] for j in range(ntp) for _ in (0, 1)], axis=0
        )

    def is_first(width):
        return lax.broadcasted_iota(jnp.int32, (2 * heads, width), 0) % (2 * hd) < hd

    logw2 = twice(logw)
    packed = jnp.where(is_first(128), logw2[:, :128], logw2[:, 128:])
    for j in range(ntp):
        lwpay[j] = packed[j * 2 * hd : (j + 1) * 2 * hd]
    lw_copies = across(lambda to: lwpay.at[to], lwall, t, ntp, "tp", lw_s, lw_r)
    lwall[t] = lwpay[t]

    lax.fori_loop(EARLY[1], nchunk, send_own, 0)

    token16 = jnp.broadcast_to(token_v[...].reshape(1, depth), (16, depth))
    new_k, new_v = project(token16)
    new_gates = lax.dot_general(wif[...], token16, over_lanes, preferred_element_type=F32)[:, 0:1]
    own_lane = lax.broadcasted_iota(jnp.int32, (hd, 128), 1)
    own_row = lax.broadcasted_iota(jnp.int32, (hd, 128), 0)
    own_pick = own_lane == t * hd + own_row

    def own_heads(row):
        column = jnp.sum(jnp.where(own_pick, row, 0.0), axis=1, keepdims=True)
        return jnp.broadcast_to(column, (hd, 128))

    own_head_col = (
        lax.broadcasted_iota(jnp.int32, (heads, hd), 0)
        == t * hd + lax.broadcasted_iota(jnp.int32, (heads, hd), 1)
    )

    def own_columns(column):
        row = jnp.sum(jnp.where(own_head_col, column, 0.0), axis=0, keepdims=True)
        return jnp.broadcast_to(row.T, (hd, 128))

    new_gate = own_columns(new_gates[0:heads])
    new_forget = own_columns(log_sigmoid(new_gates[heads:] + bias))

    cpay[0:hd, :] = own_heads(block_total)
    cpay[hd:, :] = own_heads(block_top)
    cx_copies = across(lambda to: cpay, cxs, x, nx, "sp_1", cx_s, cx_r)
    cxs[x] = cpay[...]

    own_to_sib.wait_recv()
    whole_block(xsib, sib)

    def scanned(slots, size, here):
        behind = jnp.zeros((hd, 128), F32)
        mine = behind
        peak = None
        for s in reversed(range(size)):
            level = slots[s, hd:, :] + behind
            peak = level if peak is None else jnp.maximum(peak, level)
            mine = mine + jnp.where(s > here, slots[s, 0:hd, :], 0.0)
            behind = behind + slots[s, 0:hd, :]
        return behind, peak, mine

    def landed(ref, semaphore):
        pltpu.make_async_copy(ref, ref, semaphore).wait()

    def to_sibling(g):
        return remote(
            gat.at[g, pl.ds(0, 2 * CHUNK)],
            gat.at[g, pl.ds(2 * CHUNK, 2 * CHUNK)],
            sib_s.at[g],
            sib_r.at[g],
            {"tp": sib},
        )

    def ship(g):
        landed(gat.at[g, pl.ds(0, CHUNK)], own_r.at[0, g])
        landed(gat.at[g, pl.ds(CHUNK, CHUNK)], own_r.at[1, g])
        to_sibling(g).start()

    def forward(g, side):
        part = pl.ds(side * CHUNK, CHUNK)
        return remote(
            gat.at[g, part],
            gat.at[nchunk + g // 2, part],
            fwd_s.at[g],
            own_r.at[side, nchunk + g // 2],
            {"tp": dn if side else up},
        )

    def pieces(g):
        e = g // nchunk
        c0 = g + e * (g - 2 * nchunk)
        s0 = (t + ntp - 2 - 2 * e) % ntp
        s1 = (t + 2 + 2 * e) % ntp
        return (
            s0 * rows + c0 * CHUNK,
            s1 * rows + (c0 + e) * CHUNK,
            (s0 + flip) * rows + c0 * CHUNK,
            (s1 + flip) * rows + (c0 + e) * CHUNK,
        )

    def place(lhs, starts):
        k, v = project(lhs)
        for i, start in enumerate(starts):
            at = pl.ds(pl.multiple_of(start, CHUNK), CHUNK)
            kout[at, :] = k[i * CHUNK : (i + 1) * CHUNK]
            vout[at, :] = v[i * CHUNK : (i + 1) * CHUNK]

    def from_sibling(g):
        landed(gat.at[g, pl.ds(2 * CHUNK, 2 * CHUNK)], sib_r.at[g])

    def arrive(g):
        from_sibling(g)
        place(gat[g], pieces(g))

    def near(g, carry):
        ship(g)

        @pl.when(g % 2 == 0)
        def _():
            forward(g, 0).start()

        @pl.when(g % 2 == 1)
        def _():
            forward(g, 1).start()

        @pl.when(g > 0)
        def _():
            arrive(g - 1)

        return carry

    lax.fori_loop(0, nchunk // 2, near, 0)
    for copy in cx_copies:
        copy.wait_recv()
    row_total, row_peak, later_x = scanned(cxs, nx, x)
    crow[0:hd, :] = row_total
    crow[hd:, :] = row_peak
    pl.semaphore_wait(near_z.at[1], 2)
    cz_copies = across(lambda to: crow, czs, z, nz, "sp_0", cz_s, cz_r)
    czs[z] = crow[...]
    lax.fori_loop(nchunk // 2, nchunk, near, 0)

    for copy in (*cz_copies, *lw_copies):
        copy.wait_recv()
    _, peak, later_z = scanned(czs, nz, z)
    later = later_x + later_z
    later2 = jnp.concatenate([later, later], axis=0)
    peak2 = jnp.concatenate([peak, peak], axis=0)
    stable = jnp.maximum(new_forget + peak, new_gate)
    shift = new_forget - stable
    shift2 = jnp.concatenate([shift, shift], axis=0)
    zero = jnp.zeros((hd, 128), F32)
    for s in range(ntp):
        whole = lwall[s] + later2
        tile = jnp.exp(whole - peak2)
        cwout[:, s * rows : s * rows + 128] = tile[0:hd]
        cwout[:, s * rows + 128 : (s + 1) * rows] = tile[hd:]
        tile = jnp.exp(whole + shift2)
        wread[2 * s] = jnp.concatenate([tile[0:hd], zero], axis=0)
        wread[2 * s + 1] = jnp.concatenate([tile[hd:], zero], axis=0)

    query = jnp.broadcast_to(query_v[...].reshape(1, -1), (2 * hd, nq.shape[0])).astype(F32)
    lane_head = lax.broadcasted_iota(jnp.int32, query.shape, 1) // DQK
    row_head = lax.broadcasted_iota(jnp.int32, query.shape, 0)
    queries = jnp.where(lane_head == row_head, query, 0.0)
    queries_low = queries.astype(BF16)
    acc[...] = jnp.zeros_like(acc)
    den[...] = jnp.zeros_like(den)

    def read(unit):
        at = pl.ds(pl.multiple_of(unit * 128, 128), 128)
        score = lax.dot_general(
            queries_low, kout[at, :], over_lanes, preferred_element_type=F32
        ) * (1.0 / math.sqrt(DQK))
        weighted = wread[unit] * score
        den[...] += weighted
        acc[...] += jnp.dot(weighted.astype(BF16), vout[at, :], preferred_element_type=F32)

    opposite = 4 * ((t // 2 + 2) % (ntp // 2))
    ship(nchunk)
    arrive(nchunk - 1)

    def read_near(i, carry):
        away = (i // 4) + (i // 8)
        read(4 * ((t // 2 + away) % (ntp // 2)) + i % 4)
        return carry

    lax.fori_loop(0, 12, read_near, 0)

    def far(g, carry):
        ship(g)
        arrive(g - 1)
        return carry

    lax.fori_loop(nchunk + 1, groups - 1, far, 0)
    read(opposite)
    read(opposite + 2)
    last = groups - 1
    arrive(last - 1)
    ship(last)
    ends = pieces(last)
    place(gat[last, 0 : 2 * CHUNK], ends[0:2])
    from_sibling(last)
    place(gat[last, 2 * CHUNK :], ends[2:])
    read(opposite + 1)
    read(opposite + 3)

    for h in range(hd):
        dpay[h : h + 1, :] = acc[h : h + 1, h * DV : (h + 1) * DV]
    dpay[hd:, :] = den[0:hd, :]
    dx_copies = across(lambda to: dpay, dxs, x, nx, "sp_1", dx_s, dx_r)
    dxs[x] = dpay[...]
    new_score = jnp.sum(
        queries[0:hd] * new_k[0:1, :].astype(F32), axis=1, keepdims=True
    ) * (1.0 / math.sqrt(DQK))
    own_term = jnp.exp(new_gate - stable) * new_score
    values = jnp.concatenate(
        [new_v[0:1, h * DV : (h + 1) * DV].astype(F32) for h in range(hd)], axis=0
    )
    for copy in dx_copies:
        copy.wait_recv()
    drow[...] = functools.reduce(jnp.add, [dxs[s] for s in range(nx)])
    dz_copies = across(lambda to: drow, dzs, z, nz, "sp_0", dz_s, dz_r)
    dzs[z] = drow[...]
    for copy in dz_copies:
        copy.wait_recv()
    summed = functools.reduce(jnp.add, [dzs[s] for s in range(nz)])
    numerator = summed[0:hd] + own_term * values
    denominator = jnp.sum(summed[hd:], axis=1, keepdims=True) + own_term
    rdout[...] = numerator / jnp.maximum(jnp.abs(denominator), 1.0)

    def own_left(c, carry):
        for copy in own_copies(c):
            copy.wait_send()
        return carry

    lax.fori_loop(0, nchunk, own_left, 0)

    def forwards_left(i, carry):
        forward(2 * i, 0).wait_send()
        forward(2 * i + 1, 1).wait_send()
        return carry

    lax.fori_loop(0, nchunk // 2, forwards_left, 0)

    def sibling_left(g, carry):
        to_sibling(g).wait_send()
        return carry

    lax.fori_loop(0, groups, sibling_left, 0)
    own_to_sib.wait_send()
    for copy in (*tm_copies, *lw_copies, *cx_copies, *cz_copies, *dx_copies, *dz_copies):
        copy.wait_send()


def put_out(*refs):
    sems = refs[8]
    copies = [pltpu.make_async_copy(refs[i], refs[4 + i], sems.at[i]) for i in range(4)]
    for copy in copies:
        copy.start()
    for copy in copies:
        copy.wait()


def body(
    prompt_tokens,
    key_weight,
    value_weight,
    input_weight,
    forget_weight,
    forget_bias,
    new_token,
    new_query,
):
    nz, nx, ntp = (lax.axis_size(a) for a in ("sp_0", "sp_1", "tp"))
    rows, depth = prompt_tokens.shape
    kcols, vcols = key_weight.shape[1], value_weight.shape[1]
    heads = input_weight.shape[1]
    hd = heads // ntp
    assert hd == 4 and ntp == 8 and rows == 256
    nchunk = rows // CHUNK
    groups = nchunk + nchunk // 2
    anywhere = pl.BlockSpec(memory_space=pltpu.HBM)
    vmem = pl.BlockSpec(memory_space=pltpu.VMEM)
    dma = pltpu.SemaphoreType.DMA
    tile = (2 * hd, 128)
    key_cache, value_cache, cache_weight, reading = pl.pallas_call(
        kernel,
        out_shape=(
            jax.ShapeDtypeStruct((rows * ntp, kcols), BF16),
            jax.ShapeDtypeStruct((rows * ntp, vcols), BF16),
            jax.ShapeDtypeStruct((hd, rows * ntp), F32),
            jax.ShapeDtypeStruct((hd, DV), F32),
        ),
        in_specs=[anywhere] * 8,
        out_specs=[vmem] * 4,
        scratch_shapes=[
            pltpu.VMEM((rows, depth), BF16),
            pltpu.VMEM((rows, depth), BF16),
            pltpu.VMEM((groups, 4 * CHUNK, depth), BF16),
            pltpu.VMEM((depth, kcols), BF16),
            pltpu.VMEM((depth, vcols), BF16),
            pltpu.VMEM((2 * heads, depth), BF16),
            pltpu.VMEM((heads,), F32),
            pltpu.VMEM((depth,), BF16),
            pltpu.VMEM((kcols,), BF16),
            pltpu.VMEM((2, 128), F32),
            pltpu.VMEM((ntp, 2, 128), F32),
            pltpu.VMEM((ntp, *tile), F32),
            pltpu.VMEM((ntp, *tile), F32),
            pltpu.VMEM((2 * ntp, *tile), F32),
            pltpu.VMEM(tile, F32),
            pltpu.VMEM((nx, *tile), F32),
            pltpu.VMEM(tile, F32),
            pltpu.VMEM((nz, *tile), F32),
            pltpu.VMEM(tile, F32),
            pltpu.VMEM((nx, *tile), F32),
            pltpu.VMEM(tile, F32),
            pltpu.VMEM((nz, *tile), F32),
            pltpu.VMEM((2 * hd, vcols), F32),
            pltpu.VMEM(tile, F32),
            dma((8,)),
            dma((2, nchunk)),
            dma((2, groups)),
            dma((nchunk,)),
            dma((groups,)),
            dma((groups,)),
            dma(()),
            dma(()),
            *[dma((ntp - 1,))] * 4,
            *[dma((nx - 1,))] * 2,
            *[dma((nz - 1,))] * 2,
            *[dma((nx - 1,))] * 2,
            *[dma((nz - 1,))] * 2,
            pltpu.SemaphoreType.REGULAR((2,)),
        ],
        compiler_params=pltpu.CompilerParams(
            collective_id=0, has_side_effects=True, vmem_limit_bytes=40 * 1024 * 1024
        ),
        name="prefill",
    )(
        *(
            pltpu.with_memory_space_constraint(operand, pltpu.HBM)
            for operand in (
                prompt_tokens,
                key_weight,
                value_weight,
                input_weight.T,
                forget_weight.T,
                forget_bias,
                new_token,
                new_query,
            )
        )
    )
    results = (key_cache, value_cache, cache_weight, reading)
    key_cache, value_cache, cache_weight, reading = pl.pallas_call(
        put_out,
        out_shape=tuple(jax.ShapeDtypeStruct(r.shape, r.dtype) for r in results),
        in_specs=[vmem] * 4,
        out_specs=[anywhere] * 4,
        scratch_shapes=[dma((4,))],
        compiler_params=pltpu.CompilerParams(vmem_limit_bytes=1024 * 1024),
        name="put_out",
    )(*results)
    return key_cache, value_cache, cache_weight, reading.reshape(-1)


def solution(mesh):
    torus = Mesh(mesh.devices.reshape(8, 4, mesh.shape["tp"]), ("sp_0", "sp_1", "tp"))
    return jax.shard_map(
        body,
        mesh=torus,
        in_specs=(P(SP_TP, None), P(None, "tp"), P(None, "tp"), P(), P(), P(), P(), P("tp")),
        out_specs=(P(SP, "tp"), P(SP, "tp"), P("tp", SP), P("tp")),
        check_vma=False,
    )
```

time: 60.3 us -> 59.1 us (0.980)
  Pallas kernels: 59.6 us -> 58.4 us
    pallas_call x1, Pallas kernels: 57.9 us -> 56.7 us  [body(): pl.pallas_call(kernel, out_shape=(jax.ShapeDtypeStruct((rows * ntp, kcols...]
where the time goes in v3:
time: 59.1 us; the launch traced here: 59 us
  Pallas kernels  58.4 us (99%)
  between operations  0.64 us (1%)
    pallas_call x1, Pallas kernels, body(): pl.pallas_call(kernel, out_shape=(jax.ShapeDtypeStruct((rows * ntp, kcols...  56.7 us
    pallas_call x1, Pallas kernels, body(): pl.pallas_call(put_out, out_shape=tuple((jax.ShapeDtypeStruct(r.shape, r....  1.71 us

profile of v3, /device:TPU:1, one launch (start us, length us, event | category | flops | bytes accessed | tf_op | source)
XLA Modules:
  0.0 59.0 jit_solution(12503597941905141338)
XLA Ops:
  0.6 56.7 %prefill.1 = (bf16[2048,256]{1,0:T(8,128)(2,1)S(1)}, bf16[2048,512]{1,0:T(8,128)(2,1)S(1)}, f32[4,2048]{1,0:T(4,128)S(1)}, f32[4,128]{1,0:T(4,128)S(1)}) custom-call(bf16[256,2048]{1,0:T(8,128)(2,1)} %tok.1, bf16[2048,256]{1,0:T(8,128)(2,1)} %kw.1, bf16[2048,512]{1,0:T(8,128)(2,1)} %vw.1, bf16[32,2048]{1,0:T(8,128)(2,1)} %bitcast.3, ...), custom_call_target="tpu_custom_call" | custom-call | tf_op jit(solution)/shard_map/prefill/pallas_call | solution.py:468
  57.3 1.7 %put_out.1 = (bf16[2048,256]{1,0:T(8,128)(2,1)}, bf16[2048,512]{1,0:T(8,128)(2,1)}, f32[4,2048]{1,0:T(4,128)}, f32[4,128]{1,0:T(4,128)}) custom-call(bf16[2048,256]{1,0:T(8,128)(2,1)S(1)} %get-tuple-element.12.refs_0_, bf16[2048,512]{1,0:T(8,128)(2,1)S(1)} %get-tuple-element.13.refs_1_, f32[4,2048]{1,0:T(4,128)S(1)} %get-tuple-element.14.refs_2_, ...), custom_call_target="tpu_custom_call" | custom-call | tf_op jit(solution)/shard_map/put_out/pallas_call | solution.py:538

commit v4 on v3

--- a/solution.py
+++ b/solution.py
@@ -39,8 +39,11 @@
     kout, vout, cwout, rdout,
     xown, xsib, gat, wk, wv, wif, bias_v, token_v, query_v,
     tmrow, tmall, lwpay, lwall, wread, cpay, cxs, crow, czs, dpay, dxs, drow, dzs, acc, den,
+    wko, query_far, lwsib, ypay, yfar,
     lsem, own_s, own_r, fwd_s, sib_s, sib_r, osib_s, osib_r,
     tm_s, tm_r, lw_s, lw_r, cx_s, cx_r, cz_s, cz_r, dx_s, dx_r, dz_s, dz_r, near_z,
+    over_s, over_r, a1_s, a1_r, a2_s, a2_r, b1_s, b1_r, b2_s, b2_r,
+    q_s, q_r, lwsib_s, lwsib_r, y_s, y_r,
 ):
     nz, nx, ntp = (lax.axis_size(a) for a in ("sp_0", "sp_1", "tp"))
     z, x, t = (lax.axis_index(a) for a in ("sp_0", "sp_1", "tp"))
@@ -87,6 +90,22 @@
     for d in (1, nz - 1):
         signal(near_z.at[0], "sp_0", (z + d) % nz)
 
+    far_t = (t + ntp // 2) % ntp
+    slice_rows = wko.shape[3]
+    slot = z * nx + x
+    over_copies = [
+        remote(
+            kw.at[pl.ds(pl.multiple_of((2 * slot + i) * slice_rows, slice_rows), slice_rows)],
+            wko.at[z, x, i],
+            over_s.at[i],
+            over_r.at[i],
+            {"tp": far_t},
+        )
+        for i in (0, 1)
+    ]
+    for copy in over_copies:
+        copy.start()
+
     def own_copies(c):
         piece = xown.at[pl.ds(c * CHUNK, CHUNK)]
         return (
@@ -116,6 +135,10 @@
     lax.fori_loop(0, EARLY[0], send_own, 0)
     own_to_sib = remote(xown, xsib, osib_s, osib_r, {"tp": sib})
     own_to_sib.start()
+
+    pl.semaphore_wait(near_z.at[0], 2)
+    for d in (2, nz - 2):
+        signal(near_z.at[1], "sp_0", (z + d) % nz)
 
     for load in loads[1:6]:
         load.wait()
@@ -148,11 +171,24 @@
     tm_copies = across(lambda to: tmrow, tmall, t, ntp, "tp", tm_s, tm_r)
     tmall[t] = tmrow[...]
 
+    q_copy = remote(query_v, query_far, q_s, q_r, {"tp": far_t})
+    q_copy.start()
     lax.fori_loop(EARLY[0], EARLY[1], send_own, 0)
-
-    pl.semaphore_wait(near_z.at[0], 2)
-    for d in (2, nz - 2):
-        signal(near_z.at[1], "sp_0", (z + d) % nz)
+    pl.semaphore_wait(near_z.at[1], 2)
+    for copy in over_copies:
+        copy.wait_recv()
+
+    def spread(src, dst, size, axis, here, send, recv):
+        copies = [
+            remote(src, dst, send.at[d - 1], recv.at[d - 1], {axis: (here + d) % size})
+            for d in range(1, size)
+        ]
+        for copy in copies:
+            copy.start()
+        return copies
+
+    a_first = spread(wko.at[z, x, 0], wko.at[z, x, 0], nz, "sp_0", z, a1_s, a1_r)
+    b_first = spread(wko.at[z, x, 1], wko.at[z, x, 1], nx, "sp_1", x, b1_s, b1_r)
 
     def project(lhs):
         k = jnp.dot(lhs, wk[...], preferred_element_type=F32).astype(BF16)
@@ -195,6 +231,8 @@
         lwpay[j] = packed[j * 2 * hd : (j + 1) * 2 * hd]
     lw_copies = across(lambda to: lwpay.at[to], lwall, t, ntp, "tp", lw_s, lw_r)
     lwall[t] = lwpay[t]
+    lwsib_copy = remote(lwpay.at[(sib + ntp // 2) % ntp], lwsib, lwsib_s, lwsib_r, {"tp": sib})
+    lwsib_copy.start()
 
     lax.fori_loop(EARLY[1], nchunk, send_own, 0)
 
@@ -203,10 +241,10 @@
     new_gates = lax.dot_general(wif[...], token16, over_lanes, preferred_element_type=F32)[:, 0:1]
     own_lane = lax.broadcasted_iota(jnp.int32, (hd, 128), 1)
     own_row = lax.broadcasted_iota(jnp.int32, (hd, 128), 0)
-    own_pick = own_lane == t * hd + own_row
-
-    def own_heads(row):
-        column = jnp.sum(jnp.where(own_pick, row, 0.0), axis=1, keepdims=True)
+
+    def own_heads(row, owner=t):
+        picked = own_lane == owner * hd + own_row
+        column = jnp.sum(jnp.where(picked, row, 0.0), axis=1, keepdims=True)
         return jnp.broadcast_to(column, (hd, 128))
 
     own_head_col = (
@@ -240,6 +278,20 @@
             behind = behind + slots[s, 0:hd, :]
         return behind, peak, mine
 
+    for copy in cx_copies:
+        copy.wait_recv()
+    row_total, row_peak, later_x = scanned(cxs, nx, x)
+    crow[0:hd, :] = row_total
+    crow[hd:, :] = row_peak
+    cz_copies = across(lambda to: crow, czs, z, nz, "sp_0", cz_s, cz_r)
+    czs[z] = crow[...]
+    for copy in b_first:
+        copy.wait_recv()
+    b_second = spread(wko.at[z, :, 1], wko.at[z, :, 1], nz, "sp_0", z, b2_s, b2_r)
+    for copy in a_first:
+        copy.wait_recv()
+    a_second = spread(wko.at[:, x, 0], wko.at[:, x, 0], nx, "sp_1", x, a2_s, a2_r)
+
     def landed(ref, semaphore):
         pltpu.make_async_copy(ref, ref, semaphore).wait()
 
@@ -296,13 +348,10 @@
     def near(g, carry):
         ship(g)
 
-        @pl.when(g % 2 == 0)
+        @pl.when(g == nchunk - 2)
         def _():
-            forward(g, 0).start()
-
-        @pl.when(g % 2 == 1)
-        def _():
-            forward(g, 1).start()
+            forward(0, 0).start()
+            forward(1, 1).start()
 
         @pl.when(g > 0)
         def _():
@@ -310,16 +359,48 @@
 
         return carry
 
-    lax.fori_loop(0, nchunk // 2, near, 0)
-    for copy in cx_copies:
-        copy.wait_recv()
-    row_total, row_peak, later_x = scanned(cxs, nx, x)
-    crow[0:hd, :] = row_total
-    crow[hd:, :] = row_peak
-    pl.semaphore_wait(near_z.at[1], 2)
-    cz_copies = across(lambda to: crow, czs, z, nz, "sp_0", cz_s, cz_r)
-    czs[z] = crow[...]
-    lax.fori_loop(nchunk // 2, nchunk, near, 0)
+    lax.fori_loop(0, nchunk, near, 0)
+
+    def heads_of(flat, wrapped):
+        query = jnp.broadcast_to(flat[...].reshape(1, -1), (2 * hd, nq.shape[0])).astype(F32)
+        lane_head = lax.broadcasted_iota(jnp.int32, query.shape, 1) // DQK
+        row_head = lax.broadcasted_iota(jnp.int32, query.shape, 0)
+        row_head = row_head % hd if wrapped else row_head
+        return jnp.where(lane_head == row_head, query, 0.0)
+
+    for copy in (*a_second, *b_second, q_copy, lwsib_copy):
+        copy.wait_recv()
+    queries_far = heads_of(query_far, True).astype(BF16)
+    far_top = own_heads(block_top, far_t)
+    far_weight = wko[...].reshape(depth, kw.shape[1])
+    den_far = jnp.zeros((2 * hd, 1), F32)
+    pulled = jnp.zeros((2 * hd, depth), F32)
+    for source, tile in ((xown, lwpay[far_t]), (xsib, lwsib[...])):
+        keys = jnp.dot(source[...], far_weight, preferred_element_type=F32).astype(BF16)
+        score = lax.dot_general(
+            queries_far, keys, over_lanes, preferred_element_type=F32
+        ) * (1.0 / math.sqrt(DQK))
+        level = jnp.concatenate(
+            [jnp.exp(tile[0:hd] - far_top), jnp.exp(tile[hd:] - far_top)], axis=1
+        )
+        weighted = jnp.concatenate([level, level], axis=0) * score
+        den_far = den_far + jnp.sum(weighted, axis=1, keepdims=True)
+        pulled = pulled + jnp.dot(weighted.astype(BF16), source[...], preferred_element_type=F32)
+    half = depth // 2
+    first8 = lax.broadcasted_iota(jnp.int32, (2 * hd, 1), 0) < hd
+    ypay[:, 0:half] = jnp.where(first8, pulled[:, :half], pulled[:, half:]).astype(BF16)
+    den_high = den_far.astype(BF16).astype(F32)
+    den_pair = jnp.where(first8, den_high, den_far - den_high)
+    ypay[:, half:] = jnp.broadcast_to(den_pair, (2 * hd, 128)).astype(BF16)
+    y_copy = remote(ypay, yfar, y_s, y_r, {"tp": far_t})
+    y_copy.start()
+
+    def forward_rest(i, carry):
+        forward(2 * i, 0).start()
+        forward(2 * i + 1, 1).start()
+        return carry
+
+    lax.fori_loop(1, nchunk // 2, forward_rest, 0)
 
     for copy in (*cz_copies, *lw_copies):
         copy.wait_recv()
@@ -340,10 +421,7 @@
         wread[2 * s] = jnp.concatenate([tile[0:hd], zero], axis=0)
         wread[2 * s + 1] = jnp.concatenate([tile[hd:], zero], axis=0)
 
-    query = jnp.broadcast_to(query_v[...].reshape(1, -1), (2 * hd, nq.shape[0])).astype(F32)
-    lane_head = lax.broadcasted_iota(jnp.int32, query.shape, 1) // DQK
-    row_head = lax.broadcasted_iota(jnp.int32, query.shape, 0)
-    queries = jnp.where(lane_head == row_head, query, 0.0)
+    queries = heads_of(query_v, False)
     queries_low = queries.astype(BF16)
     acc[...] = jnp.zeros_like(acc)
     den[...] = jnp.zeros_like(den)
@@ -357,38 +435,29 @@
         den[...] += weighted
         acc[...] += jnp.dot(weighted.astype(BF16), vout[at, :], preferred_element_type=F32)
 
-    opposite = 4 * ((t // 2 + 2) % (ntp // 2))
-    ship(nchunk)
-    arrive(nchunk - 1)
-
     def read_near(i, carry):
         away = (i // 4) + (i // 8)
         read(4 * ((t // 2 + away) % (ntp // 2)) + i % 4)
         return carry
 
+    arrive(nchunk - 1)
     lax.fori_loop(0, 12, read_near, 0)
-
-    def far(g, carry):
-        ship(g)
-        arrive(g - 1)
-        return carry
-
-    lax.fori_loop(nchunk + 1, groups - 1, far, 0)
-    read(opposite)
-    read(opposite + 2)
-    last = groups - 1
-    arrive(last - 1)
-    ship(last)
-    ends = pieces(last)
-    place(gat[last, 0 : 2 * CHUNK], ends[0:2])
-    from_sibling(last)
-    place(gat[last, 2 * CHUNK :], ends[2:])
-    read(opposite + 1)
-    read(opposite + 3)
+    ship(nchunk)
+    y_copy.wait_recv()
+    got_first = jnp.dot(yfar[:, 0:half], wv[0:half, :], preferred_element_type=F32)
+    got_second = jnp.dot(yfar[:, 0:half], wv[half:, :], preferred_element_type=F32)
+    got = got_first[0:hd] + got_second[hd:]
+    got_den = yfar[:, half:].astype(F32)
+    rescale = jnp.exp(own_heads(block_top) + later + shift)
 
     for h in range(hd):
-        dpay[h : h + 1, :] = acc[h : h + 1, h * DV : (h + 1) * DV]
-    dpay[hd:, :] = den[0:hd, :]
+        dpay[h : h + 1, :] = (
+            acc[h : h + 1, h * DV : (h + 1) * DV]
+            + rescale[h : h + 1] * got[h : h + 1, h * DV : (h + 1) * DV]
+        )
+    dpay[hd:, :] = den[0:hd, :] + jnp.where(
+        own_lane == 0, rescale * (got_den[0:hd] + got_den[hd:]), 0.0
+    )
     dx_copies = across(lambda to: dpay, dxs, x, nx, "sp_1", dx_s, dx_r)
     dxs[x] = dpay[...]
     new_score = jnp.sum(
@@ -398,11 +467,25 @@
     values = jnp.concatenate(
         [new_v[0:1, h * DV : (h + 1) * DV].astype(F32) for h in range(hd)], axis=0
     )
+
+    def far(g, carry):
+        ship(g)
+        arrive(g - 1)
+        return carry
+
+    lax.fori_loop(nchunk + 1, groups - 1, far, 0)
     for copy in dx_copies:
         copy.wait_recv()
     drow[...] = functools.reduce(jnp.add, [dxs[s] for s in range(nx)])
     dz_copies = across(lambda to: drow, dzs, z, nz, "sp_0", dz_s, dz_r)
     dzs[z] = drow[...]
+    last = groups - 1
+    arrive(last - 1)
+    ship(last)
+    ends = pieces(last)
+    place(gat[last, 0 : 2 * CHUNK], ends[0:2])
+    from_sibling(last)
+    place(gat[last, 2 * CHUNK :], ends[2:])
     for copy in dz_copies:
         copy.wait_recv()
     summed = functools.reduce(jnp.add, [dzs[s] for s in range(nz)])
@@ -430,7 +513,10 @@
 
     lax.fori_loop(0, groups, sibling_left, 0)
     own_to_sib.wait_send()
-    for copy in (*tm_copies, *lw_copies, *cx_copies, *cz_copies, *dx_copies, *dz_copies):
+    for copy in (
+        *tm_copies, *lw_copies, *cx_copies, *cz_copies, *dx_copies, *dz_copies,
+        *over_copies, *a_first, *a_second, *b_first, *b_second, q_copy, lwsib_copy, y_copy,
+    ):
         copy.wait_send()
 
 
@@ -500,6 +586,11 @@
             pltpu.VMEM((nz, *tile), F32),
             pltpu.VMEM((2 * hd, vcols), F32),
             pltpu.VMEM(tile, F32),
+            pltpu.VMEM((nz, nx, 2, depth // (2 * nz * nx), kcols), BF16),
+            pltpu.VMEM((kcols,), BF16),
+            pltpu.VMEM(tile, F32),
+            pltpu.VMEM((2 * hd, depth // 2 + 128), BF16),
+            pltpu.VMEM((2 * hd, depth // 2 + 128), BF16),
             dma((8,)),
             dma((2, nchunk)),
             dma((2, groups)),
@@ -514,6 +605,12 @@
             *[dma((nx - 1,))] * 2,
             *[dma((nz - 1,))] * 2,
             pltpu.SemaphoreType.REGULAR((2,)),
+            *[dma((2,))] * 2,
+            *[dma((nz - 1,))] * 2,
+            *[dma((nx - 1,))] * 2,
+            *[dma((nx - 1,))] * 2,
+            *[dma((nz - 1,))] * 2,
+            *[dma(())] * 6,
         ],
         compiler_params=pltpu.CompilerParams(
             collective_id=0, has_side_effects=True, vmem_limit_bytes=40 * 1024 * 1024

time: 59.1 us -> 55.7 us (0.942)
  Pallas kernels: 58.4 us -> 55 us
    pallas_call x1, Pallas kernels: 56.7 us -> 53.3 us  [body(): pl.pallas_call(kernel, out_shape=(jax.ShapeDtypeStruct((rows * ntp, kcols...]
where the time goes in v4:
time: 55.7 us
  Pallas kernels  55 us (99%)
  between operations  0.64 us (1%)
    pallas_call x1, Pallas kernels, body(): pl.pallas_call(kernel, out_shape=(jax.ShapeDtypeStruct((rows * ntp, kcols...  53.3 us
    pallas_call x1, Pallas kernels, body(): pl.pallas_call(put_out, out_shape=tuple((jax.ShapeDtypeStruct(r.shape, r....  1.71 us

profile of v4, /device:TPU:1, one launch (start us, length us, event | category | flops | bytes accessed | tf_op | source)
XLA Modules:
  0.0 55.7 jit_solution(8918260661585918507)
XLA Ops:
  0.6 53.3 %prefill.1 = (bf16[2048,256]{1,0:T(8,128)(2,1)S(1)}, bf16[2048,512]{1,0:T(8,128)(2,1)S(1)}, f32[4,2048]{1,0:T(4,128)S(1)}, f32[4,128]{1,0:T(4,128)S(1)}) custom-call(bf16[256,2048]{1,0:T(8,128)(2,1)} %tok.1, bf16[2048,256]{1,0:T(8,128)(2,1)} %kw.1, bf16[2048,512]{1,0:T(8,128)(2,1)} %vw.1, bf16[32,2048]{1,0:T(8,128)(2,1)} %bitcast.3, ...), custom_call_target="tpu_custom_call" | custom-call | tf_op jit(solution)/shard_map/prefill/pallas_call | solution.py:554
  54.0 1.7 %put_out.1 = (bf16[2048,256]{1,0:T(8,128)(2,1)}, bf16[2048,512]{1,0:T(8,128)(2,1)}, f32[4,2048]{1,0:T(4,128)}, f32[4,128]{1,0:T(4,128)}) custom-call(bf16[2048,256]{1,0:T(8,128)(2,1)S(1)} %get-tuple-element.12.refs_0_, bf16[2048,512]{1,0:T(8,128)(2,1)S(1)} %get-tuple-element.13.refs_1_, f32[4,2048]{1,0:T(4,128)S(1)} %get-tuple-element.14.refs_2_, ...), custom_call_target="tpu_custom_call" | custom-call | tf_op jit(solution)/shard_map/put_out/pallas_call | solution.py:635

commit v5 on v4

--- a/solution.py
+++ b/solution.py
@@ -82,13 +82,21 @@
 
     for d in range(1, ntp):
         signal(barrier, "tp", (t + d) % ntp)
-    for d in range(1, nx):
-        signal(barrier, "sp_1", (x + d) % nx)
-    for d in (1, nz - 1):
-        signal(barrier, "sp_0", (z + d) % nz)
-    pl.semaphore_wait(barrier, ntp + nx)
-    for d in (1, nz - 1):
-        signal(near_z.at[0], "sp_0", (z + d) % nz)
+
+    def along(semaphore, axis, here, size, d):
+        @pl.when(here >= d)
+        def _():
+            signal(semaphore, axis, here - d)
+
+        @pl.when(here + d < size)
+        def _():
+            signal(semaphore, axis, here + d)
+
+        return (here + size - d) // size + 1 - (here + d) // size
+
+    met = along(barrier, "sp_1", x, nx, 1) + along(barrier, "sp_0", z, nz, 1)
+    pl.semaphore_wait(barrier, ntp - 1 + met)
+    met = along(near_z.at[0], "sp_1", x, nx, 1) + along(near_z.at[0], "sp_0", z, nz, 1)
 
     far_t = (t + ntp // 2) % ntp
     slice_rows = wko.shape[3]
@@ -136,9 +144,8 @@
     own_to_sib = remote(xown, xsib, osib_s, osib_r, {"tp": sib})
     own_to_sib.start()
 
-    pl.semaphore_wait(near_z.at[0], 2)
-    for d in (2, nz - 2):
-        signal(near_z.at[1], "sp_0", (z + d) % nz)
+    pl.semaphore_wait(near_z.at[0], met)
+    met = along(near_z.at[1], "sp_1", x, nx, 2) + along(near_z.at[1], "sp_0", z, nz, 2)
 
     for load in loads[1:6]:
         load.wait()
@@ -168,13 +175,15 @@
     ).T
     tmrow[0:1, :] = pairs[0:1]
     tmrow[1:2, :] = pairs[64:65]
+    pl.semaphore_wait(near_z.at[1], met)
+    met = along(near_z.at[2], "sp_0", z, nz, 4)
     tm_copies = across(lambda to: tmrow, tmall, t, ntp, "tp", tm_s, tm_r)
     tmall[t] = tmrow[...]
 
     q_copy = remote(query_v, query_far, q_s, q_r, {"tp": far_t})
     q_copy.start()
     lax.fori_loop(EARLY[0], EARLY[1], send_own, 0)
-    pl.semaphore_wait(near_z.at[1], 2)
+    pl.semaphore_wait(near_z.at[2], met)
     for copy in over_copies:
         copy.wait_recv()
 
@@ -236,6 +245,10 @@
 
     lax.fori_loop(EARLY[1], nchunk, send_own, 0)
 
+    for copy in b_first:
+        copy.wait_recv()
+    b_second = spread(wko.at[z, :, 1], wko.at[z, :, 1], nz, "sp_0", z, b2_s, b2_r)
+
     token16 = jnp.broadcast_to(token_v[...].reshape(1, depth), (16, depth))
     new_k, new_v = project(token16)
     new_gates = lax.dot_general(wif[...], token16, over_lanes, preferred_element_type=F32)[:, 0:1]
@@ -264,6 +277,9 @@
     cx_copies = across(lambda to: cpay, cxs, x, nx, "sp_1", cx_s, cx_r)
     cxs[x] = cpay[...]
 
+    for copy in a_first:
+        copy.wait_recv()
+    a_second = spread(wko.at[:, x, 0], wko.at[:, x, 0], nx, "sp_1", x, a2_s, a2_r)
     own_to_sib.wait_recv()
     whole_block(xsib, sib)
 
@@ -285,12 +301,6 @@
     crow[hd:, :] = row_peak
     cz_copies = across(lambda to: crow, czs, z, nz, "sp_0", cz_s, cz_r)
     czs[z] = crow[...]
-    for copy in b_first:
-        copy.wait_recv()
-    b_second = spread(wko.at[z, :, 1], wko.at[z, :, 1], nz, "sp_0", z, b2_s, b2_r)
-    for copy in a_first:
-        copy.wait_recv()
-    a_second = spread(wko.at[:, x, 0], wko.at[:, x, 0], nx, "sp_1", x, a2_s, a2_r)
 
     def landed(ref, semaphore):
         pltpu.make_async_copy(ref, ref, semaphore).wait()
@@ -348,10 +358,10 @@
     def near(g, carry):
         ship(g)
 
-        @pl.when(g == nchunk - 2)
+        @pl.when(g % 2 == 1)
         def _():
-            forward(0, 0).start()
-            forward(1, 1).start()
+            forward(g - 1, 0).start()
+            forward(g, 1).start()
 
         @pl.when(g > 0)
         def _():
@@ -359,7 +369,7 @@
 
         return carry
 
-    lax.fori_loop(0, nchunk, near, 0)
+    lax.fori_loop(0, nchunk // 2, near, 0)
 
     def heads_of(flat, wrapped):
         query = jnp.broadcast_to(flat[...].reshape(1, -1), (2 * hd, nq.shape[0])).astype(F32)
@@ -368,6 +378,42 @@
         row_head = row_head % hd if wrapped else row_head
         return jnp.where(lane_head == row_head, query, 0.0)
 
+    for copy in lw_copies:
+        copy.wait_recv()
+    top = own_heads(block_top)
+    top2 = jnp.concatenate([top, top], axis=0)
+    zero = jnp.zeros((hd, 128), F32)
+    for s in range(ntp):
+        tile = jnp.exp(lwall[s] - top2)
+        wread[2 * s] = jnp.concatenate([tile[0:hd], zero], axis=0)
+        wread[2 * s + 1] = jnp.concatenate([tile[hd:], zero], axis=0)
+    queries = heads_of(query_v, False)
+    queries_low = queries.astype(BF16)
+    acc[...] = jnp.zeros_like(acc)
+    den[...] = jnp.zeros_like(den)
+
+    def read(unit):
+        at = pl.ds(pl.multiple_of(unit * 128, 128), 128)
+        score = lax.dot_general(
+            queries_low, kout[at, :], over_lanes, preferred_element_type=F32
+        ) * (1.0 / math.sqrt(DQK))
+        weighted = wread[unit] * score
+        den[...] += weighted
+        acc[...] += jnp.dot(weighted.astype(BF16), vout[at, :], preferred_element_type=F32)
+
+    def read_chip(i, carry):
+        read(4 * (t // 2) + i)
+        return carry
+
+    def read_next(i, half):
+        away = 1 + 2 * (i // 2)
+        read(4 * ((t // 2 + away) % (ntp // 2)) + 2 * (i % 2) + half)
+        return half
+
+    lax.fori_loop(0, 4, read_chip, 0)
+    lax.fori_loop(nchunk // 2, nchunk // 2 + 2, near, 0)
+    lax.fori_loop(0, 4, read_next, 0)
+    near(nchunk - 2, 0)
     for copy in (*a_second, *b_second, q_copy, lwsib_copy):
         copy.wait_recv()
     queries_far = heads_of(query_far, True).astype(BF16)
@@ -392,74 +438,47 @@
     den_high = den_far.astype(BF16).astype(F32)
     den_pair = jnp.where(first8, den_high, den_far - den_high)
     ypay[:, half:] = jnp.broadcast_to(den_pair, (2 * hd, 128)).astype(BF16)
-    y_copy = remote(ypay, yfar, y_s, y_r, {"tp": far_t})
+    y_copy = remote(ypay, yfar, y_s, y_r, {"sp_1": (x + 1) % nx, "tp": far_t})
     y_copy.start()
 
-    def forward_rest(i, carry):
-        forward(2 * i, 0).start()
-        forward(2 * i + 1, 1).start()
-        return carry
-
-    lax.fori_loop(1, nchunk // 2, forward_rest, 0)
-
-    for copy in (*cz_copies, *lw_copies):
+    near(nchunk - 1, 0)
+
+    arrive(nchunk - 1)
+    lax.fori_loop(0, 4, read_next, 1)
+    for copy in cz_copies:
         copy.wait_recv()
     _, peak, later_z = scanned(czs, nz, z)
     later = later_x + later_z
-    later2 = jnp.concatenate([later, later], axis=0)
-    peak2 = jnp.concatenate([peak, peak], axis=0)
     stable = jnp.maximum(new_forget + peak, new_gate)
     shift = new_forget - stable
-    shift2 = jnp.concatenate([shift, shift], axis=0)
-    zero = jnp.zeros((hd, 128), F32)
-    for s in range(ntp):
-        whole = lwall[s] + later2
-        tile = jnp.exp(whole - peak2)
-        cwout[:, s * rows : s * rows + 128] = tile[0:hd]
-        cwout[:, s * rows + 128 : (s + 1) * rows] = tile[hd:]
-        tile = jnp.exp(whole + shift2)
-        wread[2 * s] = jnp.concatenate([tile[0:hd], zero], axis=0)
-        wread[2 * s + 1] = jnp.concatenate([tile[hd:], zero], axis=0)
-
-    queries = heads_of(query_v, False)
-    queries_low = queries.astype(BF16)
-    acc[...] = jnp.zeros_like(acc)
-    den[...] = jnp.zeros_like(den)
-
-    def read(unit):
-        at = pl.ds(pl.multiple_of(unit * 128, 128), 128)
-        score = lax.dot_general(
-            queries_low, kout[at, :], over_lanes, preferred_element_type=F32
-        ) * (1.0 / math.sqrt(DQK))
-        weighted = wread[unit] * score
-        den[...] += weighted
-        acc[...] += jnp.dot(weighted.astype(BF16), vout[at, :], preferred_element_type=F32)
-
-    def read_near(i, carry):
-        away = (i // 4) + (i // 8)
-        read(4 * ((t // 2 + away) % (ntp // 2)) + i % 4)
-        return carry
-
-    arrive(nchunk - 1)
-    lax.fori_loop(0, 12, read_near, 0)
     ship(nchunk)
     y_copy.wait_recv()
     got_first = jnp.dot(yfar[:, 0:half], wv[0:half, :], preferred_element_type=F32)
     got_second = jnp.dot(yfar[:, 0:half], wv[half:, :], preferred_element_type=F32)
     got = got_first[0:hd] + got_second[hd:]
     got_den = yfar[:, half:].astype(F32)
-    rescale = jnp.exp(own_heads(block_top) + later + shift)
+    before = (x + nx - 1) % nx
+    _, _, later_before = scanned(cxs, nx, before)
+    rescale = jnp.exp(cxs[before, hd:, :] + later_before + later_z + shift)
+
+    rescale_near = jnp.exp(top + later + shift)
 
     for h in range(hd):
         dpay[h : h + 1, :] = (
-            acc[h : h + 1, h * DV : (h + 1) * DV]
+            rescale_near[h : h + 1] * acc[h : h + 1, h * DV : (h + 1) * DV]
             + rescale[h : h + 1] * got[h : h + 1, h * DV : (h + 1) * DV]
         )
-    dpay[hd:, :] = den[0:hd, :] + jnp.where(
+    dpay[hd:, :] = rescale_near * den[0:hd, :] + jnp.where(
         own_lane == 0, rescale * (got_den[0:hd] + got_den[hd:]), 0.0
     )
     dx_copies = across(lambda to: dpay, dxs, x, nx, "sp_1", dx_s, dx_r)
     dxs[x] = dpay[...]
+    drop = later - peak
+    drop2 = jnp.concatenate([drop, drop], axis=0)
+    for s in range(ntp):
+        tile = jnp.exp(lwall[s] + drop2)
+        cwout[:, s * rows : s * rows + 128] = tile[0:hd]
+        cwout[:, s * rows + 128 : (s + 1) * rows] = tile[hd:]
     new_score = jnp.sum(
         queries[0:hd] * new_k[0:1, :].astype(F32), axis=1, keepdims=True
     ) * (1.0 / math.sqrt(DQK))
@@ -473,12 +492,13 @@
         arrive(g - 1)
         return carry
 
-    lax.fori_loop(nchunk + 1, groups - 1, far, 0)
+    far(nchunk + 1, 0)
     for copy in dx_copies:
         copy.wait_recv()
     drow[...] = functools.reduce(jnp.add, [dxs[s] for s in range(nx)])
     dz_copies = across(lambda to: drow, dzs, z, nz, "sp_0", dz_s, dz_r)
     dzs[z] = drow[...]
+    lax.fori_loop(nchunk + 2, groups - 1, far, 0)
     last = groups - 1
     arrive(last - 1)
     ship(last)
@@ -604,7 +624,7 @@
             *[dma((nz - 1,))] * 2,
             *[dma((nx - 1,))] * 2,
             *[dma((nz - 1,))] * 2,
-            pltpu.SemaphoreType.REGULAR((2,)),
+            pltpu.SemaphoreType.REGULAR((3,)),
             *[dma((2,))] * 2,
             *[dma((nz - 1,))] * 2,
             *[dma((nx - 1,))] * 2,

time: 55.7 us -> 52.6 us (0.944)
  Pallas kernels: 55 us -> 51.8 us
    pallas_call x1, Pallas kernels: 53.3 us -> 50.1 us  [body(): pl.pallas_call(kernel, out_shape=(jax.ShapeDtypeStruct((rows * ntp, kcols...]
where the time goes in v5:
time: 52.6 us; the launch traced here: 52.5 us
  Pallas kernels  51.8 us (98%)
  between operations  0.64 us (1%)
    pallas_call x1, Pallas kernels, body(): pl.pallas_call(kernel, out_shape=(jax.ShapeDtypeStruct((rows * ntp, kcols...  50.1 us
    pallas_call x1, Pallas kernels, body(): pl.pallas_call(put_out, out_shape=tuple((jax.ShapeDtypeStruct(r.shape, r....  1.71 us

profile of v5, /device:TPU:1, one launch (start us, length us, event | category | flops | bytes accessed | tf_op | source)
XLA Modules:
  0.0 52.5 jit_solution(18083975784120393116)
XLA Ops:
  0.6 50.1 %prefill.1 = (bf16[2048,256]{1,0:T(8,128)(2,1)S(1)}, bf16[2048,512]{1,0:T(8,128)(2,1)S(1)}, f32[4,2048]{1,0:T(4,128)S(1)}, f32[4,128]{1,0:T(4,128)S(1)}) custom-call(bf16[256,2048]{1,0:T(8,128)(2,1)} %tok.1, bf16[2048,256]{1,0:T(8,128)(2,1)} %kw.1, bf16[2048,512]{1,0:T(8,128)(2,1)} %vw.1, bf16[32,2048]{1,0:T(8,128)(2,1)} %bitcast.3, ...), custom_call_target="tpu_custom_call" | custom-call | tf_op jit(solution)/shard_map/prefill/pallas_call | solution.py:574
  50.8 1.7 %put_out.1 = (bf16[2048,256]{1,0:T(8,128)(2,1)}, bf16[2048,512]{1,0:T(8,128)(2,1)}, f32[4,2048]{1,0:T(4,128)}, f32[4,128]{1,0:T(4,128)}) custom-call(bf16[2048,256]{1,0:T(8,128)(2,1)S(1)} %get-tuple-element.12.refs_0_, bf16[2048,512]{1,0:T(8,128)(2,1)S(1)} %get-tuple-element.13.refs_1_, f32[4,2048]{1,0:T(4,128)S(1)} %get-tuple-element.14.refs_2_, ...), custom_call_target="tpu_custom_call" | custom-call | tf_op jit(solution)/shard_map/put_out/pallas_call | solution.py:655

commit v6 on v5

--- a/solution.py
+++ b/solution.py
@@ -17,7 +17,7 @@
 F32 = jnp.float32
 BF16 = jnp.bfloat16
 CHUNK = 32
-EARLY = (2, 4)
+EARLY = (1, 4)
 
 
 def log_sigmoid(v):
@@ -413,7 +413,6 @@
     lax.fori_loop(0, 4, read_chip, 0)
     lax.fori_loop(nchunk // 2, nchunk // 2 + 2, near, 0)
     lax.fori_loop(0, 4, read_next, 0)
-    near(nchunk - 2, 0)
     for copy in (*a_second, *b_second, q_copy, lwsib_copy):
         copy.wait_recv()
     queries_far = heads_of(query_far, True).astype(BF16)
@@ -441,7 +440,7 @@
     y_copy = remote(ypay, yfar, y_s, y_r, {"sp_1": (x + 1) % nx, "tp": far_t})
     y_copy.start()
 
-    near(nchunk - 1, 0)
+    lax.fori_loop(nchunk - 2, nchunk, near, 0)
 
     arrive(nchunk - 1)
     lax.fori_loop(0, 4, read_next, 1)

time: 52.6 us -> 51.2 us (0.973)
  Pallas kernels: 51.8 us -> 50.4 us
    pallas_call x1, Pallas kernels: 50.1 us -> 48.7 us  [body(): pl.pallas_call(kernel, out_shape=(jax.ShapeDtypeStruct((rows * ntp, kcols...]
where the time goes in v6:
time: 51.2 us; the launch traced here: 51.1 us
  Pallas kernels  50.4 us (98%)
  between operations  0.64 us (1%)
    pallas_call x1, Pallas kernels, body(): pl.pallas_call(kernel, out_shape=(jax.ShapeDtypeStruct((rows * ntp, kcols...  48.7 us
    pallas_call x1, Pallas kernels, body(): pl.pallas_call(put_out, out_shape=tuple((jax.ShapeDtypeStruct(r.shape, r....  1.71 us

profile of v6, /device:TPU:1, one launch (start us, length us, event | category | flops | bytes accessed | tf_op | source)
XLA Modules:
  0.0 51.1 jit_solution(8056986494447284194)
XLA Ops:
  0.6 48.7 %prefill.1 = (bf16[2048,256]{1,0:T(8,128)(2,1)S(1)}, bf16[2048,512]{1,0:T(8,128)(2,1)S(1)}, f32[4,2048]{1,0:T(4,128)S(1)}, f32[4,128]{1,0:T(4,128)S(1)}) custom-call(bf16[256,2048]{1,0:T(8,128)(2,1)} %tok.1, bf16[2048,256]{1,0:T(8,128)(2,1)} %kw.1, bf16[2048,512]{1,0:T(8,128)(2,1)} %vw.1, bf16[32,2048]{1,0:T(8,128)(2,1)} %bitcast.3, ...), custom_call_target="tpu_custom_call" | custom-call | tf_op jit(solution)/shard_map/prefill/pallas_call | solution.py:573
  49.4 1.7 %put_out.1 = (bf16[2048,256]{1,0:T(8,128)(2,1)}, bf16[2048,512]{1,0:T(8,128)(2,1)}, f32[4,2048]{1,0:T(4,128)}, f32[4,128]{1,0:T(4,128)}) custom-call(bf16[2048,256]{1,0:T(8,128)(2,1)S(1)} %get-tuple-element.12.refs_0_, bf16[2048,512]{1,0:T(8,128)(2,1)S(1)} %get-tuple-element.13.refs_1_, f32[4,2048]{1,0:T(4,128)S(1)} %get-tuple-element.14.refs_2_, ...), custom_call_target="tpu_custom_call" | custom-call | tf_op jit(solution)/shard_map/put_out/pallas_call | solution.py:654

commit v7 on v6

--- a/solution.py
+++ b/solution.py
@@ -277,11 +277,11 @@
     cx_copies = across(lambda to: cpay, cxs, x, nx, "sp_1", cx_s, cx_r)
     cxs[x] = cpay[...]
 
-    for copy in a_first:
-        copy.wait_recv()
-    a_second = spread(wko.at[:, x, 0], wko.at[:, x, 0], nx, "sp_1", x, a2_s, a2_r)
     own_to_sib.wait_recv()
     whole_block(xsib, sib)
+    for copy in a_first:
+        copy.wait_recv()
+    a_second = spread(wko.at[:, x, 0], wko.at[:, x, 0], nx, "sp_1", x, a2_s, a2_r)
 
     def scanned(slots, size, here):
         behind = jnp.zeros((hd, 128), F32)
@@ -472,12 +472,6 @@
     )
     dx_copies = across(lambda to: dpay, dxs, x, nx, "sp_1", dx_s, dx_r)
     dxs[x] = dpay[...]
-    drop = later - peak
-    drop2 = jnp.concatenate([drop, drop], axis=0)
-    for s in range(ntp):
-        tile = jnp.exp(lwall[s] + drop2)
-        cwout[:, s * rows : s * rows + 128] = tile[0:hd]
-        cwout[:, s * rows + 128 : (s + 1) * rows] = tile[hd:]
     new_score = jnp.sum(
         queries[0:hd] * new_k[0:1, :].astype(F32), axis=1, keepdims=True
     ) * (1.0 / math.sqrt(DQK))
@@ -491,13 +485,18 @@
         arrive(g - 1)
         return carry
 
-    far(nchunk + 1, 0)
     for copy in dx_copies:
         copy.wait_recv()
     drow[...] = functools.reduce(jnp.add, [dxs[s] for s in range(nx)])
     dz_copies = across(lambda to: drow, dzs, z, nz, "sp_0", dz_s, dz_r)
     dzs[z] = drow[...]
-    lax.fori_loop(nchunk + 2, groups - 1, far, 0)
+    drop = later - peak
+    drop2 = jnp.concatenate([drop, drop], axis=0)
+    for s in range(ntp):
+        tile = jnp.exp(lwall[s] + drop2)
+        cwout[:, s * rows : s * rows + 128] = tile[0:hd]
+        cwout[:, s * rows + 128 : (s + 1) * rows] = tile[hd:]
+    lax.fori_loop(nchunk + 1, groups - 1, far, 0)
     last = groups - 1
     arrive(last - 1)
     ship(last)

time: 51.2 us -> 51.3 us (level)
  no operation moved by 1% of the time
where the time goes in v7:
time: 51.3 us; the launch traced here: 51.2 us
  Pallas kernels  50.6 us (99%)
  between operations  0.64 us (1%)
    pallas_call x1, Pallas kernels, body(): pl.pallas_call(kernel, out_shape=(jax.ShapeDtypeStruct((rows * ntp, kcols...  48.9 us
    pallas_call x1, Pallas kernels, body(): pl.pallas_call(put_out, out_shape=tuple((jax.ShapeDtypeStruct(r.shape, r....  1.71 us

profile of v7, /device:TPU:1, one launch (start us, length us, event | category | flops | bytes accessed | tf_op | source)
XLA Modules:
  0.0 51.2 jit_solution(16064868705098906783)
XLA Ops:
  0.6 48.9 %prefill.1 = (bf16[2048,256]{1,0:T(8,128)(2,1)S(1)}, bf16[2048,512]{1,0:T(8,128)(2,1)S(1)}, f32[4,2048]{1,0:T(4,128)S(1)}, f32[4,128]{1,0:T(4,128)S(1)}) custom-call(bf16[256,2048]{1,0:T(8,128)(2,1)} %tok.1, bf16[2048,256]{1,0:T(8,128)(2,1)} %kw.1, bf16[2048,512]{1,0:T(8,128)(2,1)} %vw.1, bf16[32,2048]{1,0:T(8,128)(2,1)} %bitcast.3, ...), custom_call_target="tpu_custom_call" | custom-call | tf_op jit(solution)/shard_map/prefill/pallas_call | solution.py:572
  49.5 1.7 %put_out.1 = (bf16[2048,256]{1,0:T(8,128)(2,1)}, bf16[2048,512]{1,0:T(8,128)(2,1)}, f32[4,2048]{1,0:T(4,128)}, f32[4,128]{1,0:T(4,128)}) custom-call(bf16[2048,256]{1,0:T(8,128)(2,1)S(1)} %get-tuple-element.12.refs_0_, bf16[2048,512]{1,0:T(8,128)(2,1)S(1)} %get-tuple-element.13.refs_1_, f32[4,2048]{1,0:T(4,128)S(1)} %get-tuple-element.14.refs_2_, ...), custom_call_target="tpu_custom_call" | custom-call | tf_op jit(solution)/shard_map/put_out/pallas_call | solution.py:653
